TPU v7x, 1024 devices: a whole 4x4x32 slice. The times are simulated.
1024 devices in a mesh: ep: 64 (over z, core), tp: 16 (over y, x).
Axes of the slice: x: 4, y: 4, z: 32, core: 2. Of those that a mesh axis runs over, the one named last changes fastest.
Arguments:
- tokens: bfloat16 [16384, 2048], P('ep'), may hold values from -6 to 6
- norm_gain: float32 [2048], replicated, may hold values from 0.1 to 1.9
- route_ids: int32 [16384, 4], P('ep'), may hold values from 0 to 127, all different within a row; in each aligned block of 256 rows (0 to 255, 256 to 511, ...) at most 12 rows name the same one
- route_weights: float32 [16384, 4], P('ep'), may hold values from 0.1 to 1
- w_gate: bfloat16 [128, 2048, 2048], P('ep', None, 'tp'), may hold values from -0.33007812 to 0.33007812
- w_up: bfloat16 [128, 2048, 2048], P('ep', None, 'tp'), may hold values from -0.33007812 to 0.33007812
- w_down: bfloat16 [128, 2048, 2048], P('ep', None, 'tp'), may hold values from -0.026489258 to 0.026489258
Outputs:
- mixed_out: bfloat16 [16384, 2048], P('ep', 'tp')
Inputs may be any that keep to these rules, and one draw needn't show every extreme that they name: `route_ids`: each token names 4 different experts. Within the tokens of one index of ep (aligned blocks of 256 tokens) no expert is named more than 12 times, a bound that some block reaches.
All inputs are finite; a program needn't handle non-finite values.
Results may differ from a plain program's by a relative error of at most 0.007.
Values may be sent and summed in bfloat16 or wider, within the bound.
No kernel may reach another device: no remote copies, remote signals or barrier semaphores. Data moves between devices by JAX's collectives and lax.ppermute only.
A program may use at most 32 MiB of HBM per device.

v0:
```python
import jax
import jax.numpy as jnp
from jax import lax
from jax.sharding import PartitionSpec as P

swiglu_limit = 7.0
swiglu_alpha = 1.702
norm_eps = 1e-05


def clamped_units(gate_pre, up_pre):
    capped = jnp.minimum(gate_pre, swiglu_limit)
    linear = jnp.clip(up_pre, -swiglu_limit, swiglu_limit)
    return capped * jax.nn.sigmoid(swiglu_alpha * capped) * (linear + 1.0)


def expert_work(outgoing, gate_weight, up_weight, down_weight):
    received = lax.all_to_all(outgoing, "ep", split_axis=1, concat_axis=1, tiled=True)
    local_count, sources, capacity, columns = received.shape
    row_count = sources * capacity
    row_block = received.reshape(local_count, row_count, columns)
    shard_piece = lax.all_gather(row_block, "tp", axis=2, tiled=True)
    gate_sum = jnp.einsum(
        "lrd,ldf->lrf", shard_piece, gate_weight, preferred_element_type=jnp.float32
    )
    up_sum = jnp.einsum("lrd,ldf->lrf", shard_piece, up_weight, preferred_element_type=jnp.float32)
    activation = clamped_units(gate_sum, up_sum).astype(jnp.bfloat16)
    out_cols = down_weight.shape[2]
    result = jnp.einsum(
        "lrf,lfd->lrd",
        lax.all_gather(activation, "tp", axis=2, tiled=True),
        down_weight,
        preferred_element_type=jnp.float32,
    )
    result = result.astype(jnp.bfloat16).reshape(local_count, sources, capacity, out_cols)
    return lax.all_to_all(result, "ep", split_axis=1, concat_axis=1, tiled=True)


def per_device(tokens, norm_gain, route_ids, route_weights, w_gate, w_up, w_down):
    local_count = w_gate.shape[0]
    sources = lax.axis_size("ep")
    tp_count = lax.axis_size("tp")
    width = tokens.shape[1]
    columns = width // tp_count
    experts = local_count * sources
    tok_rows, top_count = route_ids.shape
    capacity = 3 * tok_rows * top_count // (2 * experts)
    values = tokens.astype(jnp.float32)
    row_mean = jnp.mean(values, axis=1, keepdims=True)
    centred = values - row_mean
    row_var = jnp.mean(centred * centred, axis=1, keepdims=True)
    offset = lax.axis_index("tp") * columns
    own_cols = lax.dynamic_slice_in_dim(centred, offset, columns, 1)
    own_gain = lax.dynamic_slice_in_dim(norm_gain, offset, columns, 0)
    normed = (own_cols * lax.rsqrt(row_var + norm_eps) * own_gain).astype(jnp.bfloat16)
    flat_ids = route_ids.reshape(-1)
    matches = (flat_ids[:, None] == jnp.arange(experts, dtype=jnp.int32)[None, :]).astype(jnp.int32)
    earlier = jnp.cumsum(matches, axis=0) - matches
    slot_index = jnp.sum(earlier * matches, axis=1)
    position = (
        flat_ids % local_count * (sources * capacity)
        + flat_ids // local_count * capacity
        + slot_index
    )
    buffer_rows = local_count * sources * capacity
    placed = (
        position.reshape(tok_rows, top_count)[:, :, None]
        == jnp.arange(buffer_rows, dtype=jnp.int32)[None, None, :]
    )
    placement_matrix = jnp.any(placed, axis=1).astype(jnp.bfloat16)
    outgoing = jnp.einsum("tp,td->pd", placement_matrix, normed, preferred_element_type=jnp.float32)
    outgoing = outgoing.astype(jnp.bfloat16).reshape(local_count, sources, capacity, columns)
    returned = expert_work(outgoing, w_gate, w_up, w_down)
    flat_out = returned.reshape(buffer_rows, columns)
    picked = flat_out[position].reshape(tok_rows, top_count, columns).astype(jnp.float32)
    return jnp.sum(picked * route_weights[:, :, None], axis=1).astype(jnp.bfloat16)


def solution(mesh):
    return jax.shard_map(
        per_device,
        mesh=mesh,
        in_specs=(
            P("ep", None),
            P(),
            P("ep", None),
            P("ep", None),
            P("ep", None, "tp"),
            P("ep", None, "tp"),
            P("ep", None, "tp"),
        ),
        out_specs=P("ep", "tp"),
        check_vma=False,
    )
```

profile of v0, /device:TPU:1, one launch (start us, length us, event | category | flops | bytes accessed | tf_op | source)
XLA Modules:
  0.0 392.6 jit_solution(15387578315174305796)
XLA Ops:
  6.5 0.9 copy.62
  7.4 0.1 eq.44
  7.6 0.1 eq.40
  7.7 1.4 convert_reduce_fusion
  9.1 0.1 copy.64
  9.3 0.2 fusion.7
  9.5 0.1 copy.65
  9.7 0.4 fusion.6
  10.0 0.1 reduce_sum.41
  10.2 0.1 copy.66
  10.2 0.7 fusion.14
  11.0 1.7 fusion
  12.7 1.6 multiply_reduce_fusion
  14.3 0.8 dynamic_slice.7
  15.1 2.4 convolution_convert_fusion
  17.5 1.2 reshape.204
  18.7 0.4 copy.67
  19.1 83.4 %all_to_all.10 = bf16[2,64,12,128]{3,0,2,1:T(2,128)(2,1)S(1)} all-to-all(bf16[2,64,12,128]{3,0,2,1:T(2,128)(2,1)S(1)} %copy.67), channel_id=1, replica_groups=mesh['ep'=64,'tp'=16] {'ep'}, dimensions={1} | all-to-all | bytes 786432 | tf_op jit(solution)/shard_map/all_to_all | solution.py:18
  102.5 0.8 copy.68
  103.4 83.6 %all-gather.3.cloned.1.call-done = bf16[2,768,2048]{2,1,0:T(8,128)(2,1)} async-done(((bf16[2,768,128]{2,1,0:T(8,128)(2,1)}), bf16[2,768,2048]{2,1,0:T(8,128)(2,1)}) %all-gather.3.cloned.1.call-update) | async-done | bytes 6291472 | tf_op jit(solution)/shard_map/all_gather | solution.py:22
  187.0 4.7 %convolution_minimum_fusion = f32[2,768,128]{2,1,0:T(8,128)S(1)} fusion(bf16[2,768,2048]{2,1,0:T(8,128)(2,1)} %all-gather.3.cloned.1.call-done, bf16[2,2048,128]{2,1,0:T(8,128)(2,1)S(1)} %copy-done), kind=kOutput, calls=%fused_computation.8 | convolution fusion | flops 805502976 | bytes 8126464 | tf_op jit(solution)/shard_map/lrd,ldf->lrf/dot_general | solution.py:23
  191.8 2.6 fusion.3
  194.4 102.5 %all-gather.5.cloned.1.call-done = bf16[2,768,2048]{2,1,0:T(8,128)(2,1)} async-done(((bf16[2,768,128]{2,1,0:T(8,128)(2,1)}), bf16[2,768,2048]{2,1,0:T(8,128)(2,1)}) %all-gather.5.cloned.1.call-update) | async-done | bytes 6291472 | tf_op jit(solution)/shard_map/all_gather | solution.py:31
  296.9 4.8 %convolution_convert_fusion.1 = bf16[2,768,128]{2,1,0:T(8,128)(2,1)S(1)} fusion(bf16[2,768,2048]{2,1,0:T(8,128)(2,1)} %all-gather.5.cloned.1.call-done, bf16[2,2048,128]{2,1,0:T(8,128)(2,1)} %param.13), kind=kOutput, calls=%fused_computation.12 | convolution fusion | flops 805502976 | bytes 7733248 | tf_op jit(solution)/shard_map/lrf,lfd->lrd/dot_general | solution.py:29
  301.8 1.1 copy.69
  302.9 25.1 %all-to-all-start.1 = ((bf16[2,64,12,128]{3,0,2,1:T(2,128)(2,1)}), bf16[2,64,12,128]{3,0,2,1:T(2,128)(2,1)S(1)}, u32[]{:S(2)}, u32[]{:S(2)}) async-start(bf16[2,64,12,128]{3,0,2,1:T(2,128)(2,1)} %bitcast.4), calls=%async_computation.1 | async-start | bytes 786432 | tf_op jit(solution)/shard_map/all_to_all | solution.py:36
  328.0 0.1 reshape.208
  328.2 0.1 copy.72
  328.4 52.9 %all-to-all-done.1 = bf16[2,64,12,128]{3,0,2,1:T(2,128)(2,1)S(1)} async-done(((bf16[2,64,12,128]{3,0,2,1:T(2,128)(2,1)}), bf16[2,64,12,128]{3,0,2,1:T(2,128)(2,1)S(1)}, u32[]{:S(2)}, u32[]{:S(2)}) %all-to-all-start.1) | async-done | bytes 393248 | tf_op jit(solution)/shard_map/all_to_all | solution.py:36
  381.3 0.1 reshape.207
  381.4 3.2 gather_fusion
  384.7 1.1 fusion.4
  (21 shorter events, 0.3 us)
Async XLA Ops:
  6.5 180.5 %copy-start = (bf16[2,2048,128]{2,1,0:T(8,128)(2,1)S(1)}, bf16[2,2048,128]{2,1,0:T(8,128)(2,1)}, u32[]{:S(2)}) copy-start(bf16[2,2048,128]{2,1,0:T(8,128)(2,1)} %param.11) | copy-start | bytes 3145732
  6.5 180.5 %all-gather.3.cloned.1.call-start = ((), (), s32[]{:S(2)}) async-start(), calls=%async_computation.2 | async-start | bytes 6684672 | tf_op jit(solution)/shard_map/all_gather | solution.py:22
  17.5 174.2 %copy-start.3 = (bf16[2,2048,128]{2,1,0:T(8,128)(2,1)S(1)}, bf16[2,2048,128]{2,1,0:T(8,128)(2,1)}, u32[]{:S(2)}) copy-start(bf16[2,2048,128]{2,1,0:T(8,128)(2,1)} %param.12) | copy-start | bytes 3145732
  103.4 193.6 %all-gather.5.cloned.1.call-start = ((), (), s32[]{:S(2)}) async-start(), calls=%async_computation.3 | async-start | bytes 6684672 | tf_op jit(solution)/shard_map/all_gather | solution.py:31
  187.0 4.7 %copy-start.1 = (bf16[2,768,2048]{2,1,0:T(8,128)(2,1)S(1)}, bf16[2,768,2048]{2,1,0:T(8,128)(2,1)}, u32[]{:S(2)}) copy-start(bf16[2,768,2048]{2,1,0:T(8,128)(2,1)} %all-gather.3.cloned.1.call-done) | copy-start | bytes 18874372
  194.4 133.8 %copy-start.2 = (f32[256,4]{0,1:T(4,128)S(1)}, f32[256,4]{0,1:T(4,128)}, u32[]{:S(2)}) copy-start(f32[256,4]{0,1:T(4,128)} %param.10) | copy-start | bytes 12292
  302.9 78.4 %all-to-all-start.1 = ((bf16[2,64,12,128]{3,0,2,1:T(2,128)(2,1)}), bf16[2,64,12,128]{3,0,2,1:T(2,128)(2,1)S(1)}, u32[]{:S(2)}, u32[]{:S(2)}) async-start(bf16[2,64,12,128]{3,0,2,1:T(2,128)(2,1)} %bitcast.4), calls=%async_computation.1 | async-start | bytes 786432 | tf_op jit(solution)/shard_map/all_to_all | solution.py:36
Sparse Core Ops, SparseCore 0:
  103.5 83.4 all-gather.2
  194.5 102.3 all-gather.4
where the time goes:
time: 393 us
  waiting for transfers between devices  239 us (61%)
  blocking collectives  83.4 us (21%)
  starting transfers between devices  25.2 us (6%)
  matrix products  14.6 us (4%)
  between operations  13.6 us (3%)
  local copies, waits for them, and re-layouts  9.52 us (2%)
  other arithmetic  7.28 us (2%)
    all_gather x1, waiting for transfers between devices, expert_work(): lax.all_gather(activation, 'tp', axis=2, tiled=True)  103 us
    all_gather x1, waiting for transfers between devices, expert_work(): shard_piece = lax.all_gather(row_block, 'tp', axis=2, tiled=True)  83.6 us
    all_to_all x1, blocking collectives, expert_work(): lax.all_to_all(outgoing, 'ep', split_axis=1, concat_axis=1, tiled=True)  83.4 us
    all_to_all x1, waiting for transfers between devices, expert_work(): return lax.all_to_all(result, 'ep', split_axis=1, concat_axis=1, tiled=True)  52.9 us
    all_to_all x1, starting transfers between devices, expert_work(): return lax.all_to_all(result, 'ep', split_axis=1, concat_axis=1, tiled=True)  25.1 us
  transfers between devices with their start and end apart: 3, of which 3 were waited for; matrix products, arithmetic and copies ran while one was open for 0% of the time, Pallas kernels for 0%

commit v1 on v0

v1 whole, which is shorter than its diff:
```python
import jax
import jax.numpy as jnp
import numpy as np
from jax import lax
from jax.experimental import pallas as pl
from jax.experimental.pallas import tpu as pltpu
from jax.sharding import PartitionSpec as P

swiglu_limit = 7.0
swiglu_alpha = 1.702
norm_eps = 1e-05

CHIPS = 32
SIDE = 4
PLANE = SIDE * SIDE
CAP = 12
TOK = 256
ROWS = CHIPS * CAP
UNIT = 2 * CAP
SLAB = SIDE * CAP
HALF = 1024
LANES = 128
BLOCK = SIDE * LANES
BF = jnp.bfloat16
F32 = jnp.float32


def clamped_units(gate_pre, up_pre):
    capped = jnp.minimum(gate_pre, swiglu_limit)
    linear = jnp.clip(up_pre, -swiglu_limit, swiglu_limit)
    return capped * jax.nn.sigmoid(swiglu_alpha * capped) * (linear + 1.0)


def iota(shape, dim):
    return lax.broadcasted_iota(jnp.int32, shape, dim)


def as_bf(mask):
    return jnp.where(mask, 1.0, 0.0).astype(BF)


def prep_kernel(pos_ref, tok_ref, gain_ref, ids_ref, out0_ref, out1_ref):
    values = tok_ref[...].astype(F32)
    row_mean = jnp.mean(values, axis=1, keepdims=True)
    centred = values - row_mean
    row_var = jnp.mean(centred * centred, axis=1, keepdims=True)
    normed = (centred * lax.rsqrt(row_var + norm_eps) * gain_ref[...]).astype(BF)
    shape = (2 * SIDE * UNIT, TOK)
    r = iota(shape, 0)
    second = r >= SIDE * UNIT
    rest = jnp.where(second, r - SIDE * UNIT, r)
    q = (rest * 2731) >> 16
    rest = rest - q * UNIT
    half = rest >= CAP
    slot = jnp.where(half, rest - CAP, rest)
    name = jnp.where(second, pos_ref[4], pos_ref[3]) * SIDE + q
    named = name == ids_ref[0:1, :]
    for k in range(1, 4):
        named = named | (name == ids_ref[k : k + 1, :])
    before = as_bf(iota((TOK, TOK), 0) < iota((TOK, TOK), 1))
    rank = jnp.dot(as_bf(named), before, preferred_element_type=F32)
    placed = as_bf(named & (rank == slot.astype(F32)))
    wide = jnp.dot(placed, normed, preferred_element_type=F32)
    upper = half[:, :1]
    out = jnp.where(upper, wide[:, HALF:], wide[:, :HALF]).astype(BF)
    out0_ref[...] = out[: SIDE * UNIT]
    out1_ref[...] = out[SIDE * UNIT :]


def scale_kernel(ids_ref, weight_ref, out_ref):
    shape = (TOK, 4 * ROWS)
    r = iota(shape, 1)
    name = (r * 5462) >> 16
    slot = r - name * CAP
    named = jnp.zeros(shape, jnp.bool_)
    scale = jnp.zeros(shape, F32)
    for k in range(4):
        hit = name == ids_ref[:, k : k + 1]
        named = named | hit
        scale = jnp.where(hit, weight_ref[:, k : k + 1], scale)
    before = as_bf(iota((TOK, TOK), 1) < iota((TOK, TOK), 0))
    rank = jnp.dot(before, as_bf(named), preferred_element_type=F32)
    scale = jnp.where(named & (rank == slot.astype(F32)), scale, 0.0)
    high = scale.astype(BF)
    out_ref[0] = high
    out_ref[1] = (scale - high.astype(F32)).astype(BF)


def combine_kernel(scale_ref, ret_ref, out_ref):
    back = ret_ref[...]
    total = jnp.dot(scale_ref[0], back, preferred_element_type=F32)
    total += jnp.dot(scale_ref[1], back, preferred_element_type=F32)
    out_ref[...] = total.astype(BF)


GROUP = 4


def unpack_matrix():
    n = GROUP * 2 * UNIT
    q = np.arange(n)
    half, unit, slot = q // (n // 2), q % (n // 2) // CAP, q % CAP
    m = np.zeros((n, n), np.float32)
    m[q, unit * UNIT + half * CAP + slot] = 1.0
    return m


def pack_matrix():
    n = GROUP * SLAB
    q = np.arange(n)
    unit, cb, slot = q // SLAB, q % SLAB // CAP, q % CAP
    m = np.zeros((n, n), np.float32)
    m[q, cb * SLAB + unit * CAP + slot] = 1.0
    return m


def gate_up_kernel(pos_ref, perm_ref, raw_ref, w0, w1, v0, v1, act_ref, xs):
    core, x = pos_ref[0], pos_ref[1]
    n = GROUP * 2 * UNIT
    for g in range(PLANE // GROUP):
        part = jnp.dot(
            perm_ref[...], raw_ref[g * n : (g + 1) * n, :], preferred_element_type=F32
        ).astype(BF)
        rows = slice(g * n // 2, (g + 1) * n // 2)
        xs[rows, :HALF] = part[: n // 2]
        xs[rows, HALF:] = part[n // 2 :]
    for k, (own, w) in enumerate(((1, w0), (1, w1), (0, v0), (0, v1))):
        both = jnp.concatenate([w[0], w[1]], axis=1)
        pre = jnp.dot(xs[...], both, preferred_element_type=F32)
        block = clamped_units(pre[:, :LANES], pre[:, LANES:]).astype(BF)
        col = 2 * ((x + k) % 2) + (core if own else 1 - core)
        cols = pl.ds(pl.multiple_of(col * LANES, LANES), LANES)
        for i in range(SIDE):
            act_ref[i, :, cols] = block


def down_kernel(pos_ref, perm_ref, acts, d0, d1, e0, e1, out_ref, res):
    core, x, z = pos_ref[0], pos_ref[1], pos_ref[2]
    for own, pair in ((1, (d0, d1)), (0, (e0, e1))):
        total = jnp.zeros((ROWS, 2 * LANES), F32)
        for i in range(SIDE):
            rows = slice(i * BLOCK, (i + 1) * BLOCK)
            both = jnp.concatenate([pair[0][rows, :], pair[1][rows, :]], axis=1)
            total += jnp.dot(acts[i], both, preferred_element_type=F32)
        out = total.astype(BF)
        for k in range(2):
            col = 2 * ((x + k) % 2) + (core if own else 1 - core)
            cols = pl.ds(pl.multiple_of(col * LANES, LANES), LANES)
            res[:, cols] = out[:, k * LANES : (k + 1) * LANES]
    sign = 1 - 2 * core
    for g in range(CHIPS // GROUP):
        rows = slice(g * SLAB, (g + 1) * SLAB)
        part = jnp.concatenate(
            [res[rows, cb * LANES : (cb + 1) * LANES] for cb in range(SIDE)], axis=0
        )
        part = jnp.dot(perm_ref[...], part, preferred_element_type=F32).astype(BF)
        for i in range(GROUP):
            t, m = divmod(g * GROUP + i, 2)
            shift = sign * (-(15 - t) if m else t + 1)
            source = (z - shift + 2 * CHIPS) % CHIPS
            out_ref[pl.ds(pl.multiple_of(source * SLAB, SLAB), SLAB), :] = part[
                i * SLAB : (i + 1) * SLAB
            ]


def call(kernel, out_shape, n_in, flops, nbytes, scratch=(), scalars=True):
    vmem = pl.BlockSpec(memory_space=pltpu.VMEM)
    first = [pl.BlockSpec(memory_space=pltpu.SMEM)] if scalars else []
    return pl.pallas_call(
        kernel,
        out_shape=out_shape,
        in_specs=first + [vmem] * (n_in - len(first)),
        out_specs=jax.tree.map(lambda _: vmem, out_shape),
        scratch_shapes=list(scratch),
        compiler_params=pltpu.CompilerParams(vmem_limit_bytes=24 * 2**20),
        cost_estimate=pl.CostEstimate(
            flops=flops, bytes_accessed=nbytes, transcendentals=0
        ),
    )


def devices():
    for z in range(CHIPS):
        for c in range(2):
            for y in range(SIDE):
                for x in range(SIDE):
                    yield z, c, y, x


def at(z, c, y, x):
    return (2 * (z % CHIPS) + c) * PLANE + SIDE * y + x


def shift_of(m, c, t):
    s = -(15 - t) if m else t + 1
    return s if c == 0 else -s


def z_pairs(m):
    return [
        (at(z, c, y, x), at(z + shift_of(m, c, SIDE * y + x), c, y, x))
        for z, c, y, x in devices()
    ]


def weight_pairs(k):
    return [
        (at(z, c, y, x), at(z, x % 2, y, 2 * c + (x // 2 + k) % 2))
        for z, c, y, x in devices()
    ]


SIBLING = [(at(z, c, y, x), at(z, 1 - c, y, x)) for z, c, y, x in devices()]
Y_GROUPS = [[SIDE * y + x for y in range(SIDE)] for x in range(SIDE)]
BACK_GROUPS = [
    [at(z, c, y, x) for z in range(CHIPS) for x in range(SIDE)]
    for c in range(2)
    for y in range(SIDE)
]
BOTH = ("ep", "tp")


def permute(a, pairs):
    return lax.ppermute(a, BOTH, pairs)


def per_device(tokens, norm_gain, route_ids, route_weights, w_gate, w_up, w_down):
    tp, ep = lax.axis_index("tp"), lax.axis_index("ep")
    x, z, core = tp & 3, ep >> 1, ep & 1
    sign = 1 - 2 * core
    pos = jnp.stack(
        [core, x, z, (z + sign * (tp + 1)) & 31, (z - sign * (15 - tp)) & 31]
    ).astype(jnp.int32)

    message = jax.ShapeDtypeStruct((SIDE * UNIT, HALF), BF)
    out0, out1 = call(prep_kernel, (message, message), 4, 10**8, 2 * 10**6)(
        pos, tokens, norm_gain.reshape(1, -1), route_ids.T
    )
    got = [permute(out, z_pairs(m)) for m, out in enumerate((out0, out1))]

    def pick(w, i):
        return lax.dynamic_index_in_dim(w, i, 0, keepdims=False)

    def share(blocks):
        own = [permute(blocks[k], weight_pairs(k)) for k in range(2)]
        return own + [permute(b, SIBLING) for b in own]

    mine = (tp >> 1) & 1
    gu_blocks = share(
        [jnp.stack([pick(w_gate, i), pick(w_up, i)]) for i in (mine, 1 - mine)]
    )
    wd_blocks = share([pick(w_down, i) for i in (mine, 1 - mine)])
    scale = call(
        scale_kernel,
        jax.ShapeDtypeStruct((2, TOK, 4 * ROWS), BF),
        2,
        10**8,
        2 * 10**6,
        scalars=False,
    )(route_ids, route_weights)

    units = jnp.concatenate([g.reshape(SIDE, UNIT, HALF) for g in got], axis=1)
    units = jnp.broadcast_to(units[None], (SIDE, SIDE, 2 * UNIT, HALF))
    raw = lax.all_to_all(
        units.reshape(PLANE, 2 * UNIT, HALF), "tp", 0, 0, tiled=True
    ).reshape(2 * ROWS, HALF)
    act = call(
        gate_up_kernel,
        jax.ShapeDtypeStruct((SIDE, ROWS, BLOCK), BF),
        7,
        2 * 10**9,
        6 * 10**6,
        [pltpu.VMEM((ROWS, 2 * HALF), BF)],
    )(pos, jnp.asarray(unpack_matrix(), BF), raw, *gu_blocks)
    acts = lax.all_to_all(act, "tp", 0, 0, tiled=True, axis_index_groups=Y_GROUPS)
    result = call(
        down_kernel,
        jax.ShapeDtypeStruct((4 * ROWS, LANES), BF),
        7,
        10**9,
        4 * 10**6,
        [pltpu.VMEM((ROWS, BLOCK), BF)],
    )(pos, jnp.asarray(pack_matrix(), BF), acts, *wd_blocks)
    returned = lax.all_to_all(
        result.reshape(4 * CHIPS, 3, 4, LANES),
        BOTH,
        0,
        0,
        tiled=True,
        axis_index_groups=BACK_GROUPS,
    ).reshape(4 * ROWS, LANES)
    return call(
        combine_kernel,
        jax.ShapeDtypeStruct((TOK, LANES), BF),
        2,
        2 * 10**8,
        2 * 10**6,
        scalars=False,
    )(scale, returned)


def solution(mesh):
    return jax.shard_map(
        per_device,
        mesh=mesh,
        in_specs=(
            P("ep", None),
            P(),
            P("ep", None),
            P("ep", None),
            P("ep", None, "tp"),
            P("ep", None, "tp"),
            P("ep", None, "tp"),
        ),
        out_specs=P("ep", "tp"),
        check_vma=False,
    )
```

time: 393 us -> 222 us (0.56)
  the two profiles are of different devices: /device:TPU:1 before, /device:TPU:14 now
where the time goes in v1:
time: 222 us; the launch traced here: 221 us
  waiting for transfers between devices  110 us (50%)
  starting transfers between devices  91.4 us (41%)
  Pallas kernels  12.5 us (6%)
  local copies, waits for them, and re-layouts  5.31 us (2%)
    all_to_all x1, waiting for transfers between devices, per_device(): lax.all_to_all(result.reshape(4 * CHIPS, 3, 4, LANES), BOTH, 0, 0, tiled=...  51 us
    ppermute x10, starting transfers between devices, permute(): return lax.ppermute(a, BOTH, pairs)  47.9 us
    ppermute x10, waiting for transfers between devices, permute(): return lax.ppermute(a, BOTH, pairs)  42.9 us
    all_to_all x1, starting transfers between devices, per_device(): lax.all_to_all(result.reshape(4 * CHIPS, 3, 4, LANES), BOTH, 0, 0, tiled=...  27.5 us
    all_to_all x1, waiting for transfers between devices, per_device(): lax.all_to_all(units.reshape(PLANE, 2 * UNIT, HALF), 'tp', 0, 0, tiled=True)  15.9 us
    all_to_all x1, starting transfers between devices, per_device(): lax.all_to_all(units.reshape(PLANE, 2 * UNIT, HALF), 'tp', 0, 0, tiled=True)  12 us
    pallas_call x1, Pallas kernels, per_device(): call(gate_up_kernel, jax.ShapeDtypeStruct((SIDE, ROWS, BLOCK), BF), 7, 2...  5.4 us
  transfers between devices with their start and end apart: 13, of which 7 were waited for; matrix products, arithmetic and copies ran while one was open for 1% of the time, Pallas kernels for 1%

profile of v1, /device:TPU:14, one launch (start us, length us, event | category | flops | bytes accessed | tf_op | source)
XLA Modules:
  0.0 221.4 jit_solution(424586961976114817)
XLA Ops:
  0.0 1.7 constant_dynamic-slice_fusion
  1.7 1.1 pad_maximum_fusion
  2.7 2.9 %collective-permute-start.2 = (bf16[2,2048,128]{2,1,0:T(8,128)(2,1)}, bf16[2,2048,128]{2,1,0:T(8,128)(2,1)S(1)}, u32[]{:S(2)}, u32[]{:S(2)}) collective-permute-start(bf16[2,2048,128]{2,1,0:T(8,128)(2,1)} %pad_maximum_fusion), channel_id=1, source_target_pairs={{0,0},{1,16},{2,1},{3,17},{4,4},{5,20},{6,5},{7,21},{8,8},{9,24},{... | collective-permute-start | bytes 3145736 | tf_op jit(solution)/shard_map/ppermute | solution.py:224
  5.6 1.1 pad_maximum_fusion.1
  6.7 4.3 %collective-permute-start.3 = (bf16[2,2048,128]{2,1,0:T(8,128)(2,1)}, bf16[2,2048,128]{2,1,0:T(8,128)(2,1)}, u32[]{:S(2)}, u32[]{:S(2)}) collective-permute-start(bf16[2,2048,128]{2,1,0:T(8,128)(2,1)} %pad_maximum_fusion.1), channel_id=1, source_target_pairs={{0,1},{1,17},{2,0},{3,16},{4,5},{5,21},{6,4},{7,20},{8,9},{9,25},{... | collective-permute-start | bytes 3145736 | tf_op jit(solution)/shard_map/ppermute | solution.py:224
  11.1 1.6 shard_map.92
  12.6 15.7 %collective-permute-start = (bf16[96,1024]{1,0:T(8,128)(2,1)S(1)}, bf16[96,1024]{1,0:T(8,128)(2,1)S(1)}, u32[]{:S(2)}, u32[]{:S(2)}) collective-permute-start(bf16[96,1024]{1,0:T(8,128)(2,1)S(1)} %get-tuple-element.7), channel_id=1, source_target_pairs={{0,32},{1,65},{2,98},{3,131},{4,164},{5,197},{6,230},{7,263},{8,29... | collective-permute-start | bytes 589832 | tf_op jit(solution)/shard_map/ppermute | solution.py:224
  28.4 9.2 %collective-permute-start.1 = (bf16[96,1024]{1,0:T(8,128)(2,1)S(1)}, bf16[96,1024]{1,0:T(8,128)(2,1)S(1)}, u32[]{:S(2)}, u32[]{:S(2)}) collective-permute-start(bf16[96,1024]{1,0:T(8,128)(2,1)S(1)} %get-tuple-element.8), channel_id=1, source_target_pairs={{0,544},{1,577},{2,610},{3,643},{4,676},{5,709},{6,742},{7,775},{8... | collective-permute-start | bytes 589832 | tf_op jit(solution)/shard_map/ppermute | solution.py:224
  37.6 2.3 %collective-permute-done = bf16[96,1024]{1,0:T(8,128)(2,1)S(1)} collective-permute-done((bf16[96,1024]{1,0:T(8,128)(2,1)S(1)}, bf16[96,1024]{1,0:T(8,128)(2,1)S(1)}, u32[]{:S(2)}, u32[]{:S(2)}) %collective-permute-start) | collective-permute-done | bytes 196640 | tf_op jit(solution)/shard_map/ppermute | solution.py:224
  39.9 28.4 %collective-permute-done.1 = bf16[96,1024]{1,0:T(8,128)(2,1)S(1)} collective-permute-done((bf16[96,1024]{1,0:T(8,128)(2,1)S(1)}, bf16[96,1024]{1,0:T(8,128)(2,1)S(1)}, u32[]{:S(2)}, u32[]{:S(2)}) %collective-permute-start.1) | collective-permute-done | bytes 196640 | tf_op jit(solution)/shard_map/ppermute | solution.py:224
  68.4 1.4 broadcast_in_dim.2
  69.7 12.0 %all-to-all-start = ((bf16[16,48,1024]{2,1,0:T(8,128)(2,1)}), bf16[16,48,1024]{2,1,0:T(8,128)(2,1)S(1)}, u32[]{:S(2)}, u32[]{:S(2)}) async-start(bf16[16,48,1024]{2,1,0:T(8,128)(2,1)} %bitcast.21), calls=%async_computation | async-start | bytes 3145728 | tf_op jit(solution)/shard_map/all_to_all | solution.py:264
  81.8 1.9 collective-permute-start.4
  83.7 2.4 %collective-permute-start.5 = (bf16[2,2048,128]{2,1,0:T(8,128)(2,1)}, bf16[2,2048,128]{2,1,0:T(8,128)(2,1)}, u32[]{:S(2)}, u32[]{:S(2)}) collective-permute-start(bf16[2,2048,128]{2,1,0:T(8,128)(2,1)} %collective-permute-done.3.w1), channel_id=1, source_target_pairs={{0,16},{1,17},{2,18},{3,19},{4,20},{5,21},{6,22},{7,23},{8,24},{9,... | collective-permute-start | bytes 3145736 | tf_op jit(solution)/shard_map/ppermute | solution.py:224
  86.1 15.9 %all-to-all-done = bf16[16,48,1024]{2,1,0:T(8,128)(2,1)S(1)} async-done(((bf16[16,48,1024]{2,1,0:T(8,128)(2,1)}), bf16[16,48,1024]{2,1,0:T(8,128)(2,1)S(1)}, u32[]{:S(2)}, u32[]{:S(2)}) %all-to-all-start) | async-done | bytes 1572896 | tf_op jit(solution)/shard_map/all_to_all | solution.py:264
  102.0 5.4 %shard_map.93 = bf16[4,384,512]{2,1,0:T(8,128)(2,1)} custom-call(s32[5]{0:T(128)S(1)} %stack.33.pos_ref, bf16[192,192]{1,0:T(8,128)(2,1)S(1)} %copy-done.3, bf16[768,1024]{1,0:T(8,128)(2,1)S(1)} %bitcast.17, bf16[2,2048,128]{2,1,0:T(8,128)(2,1)S(1)} %collective-permute-done.2.w0, bf16[2,2048,128]{2,1,0:T(8,128)(2,1)} %collective-permute-done.3.w1, ...), custom_call_target="tpu_custom_call" | custom-call | flops 2000000000 | bytes 6000000 | tf_op jit(solution)/shard_map/pallas_call | solution.py:267
  107.4 4.1 %all-to-all-start.1 = ((bf16[4,384,512]{2,1,0:T(8,128)(2,1)}), bf16[4,384,512]{2,1,0:T(8,128)(2,1)S(1)}, u32[]{:S(2)}, u32[]{:S(2)}) async-start(bf16[4,384,512]{2,1,0:T(8,128)(2,1)} %shard_map.93), calls=%async_computation.1 | async-start | bytes 3145728 | tf_op jit(solution)/shard_map/all_to_all | solution.py:275
  111.6 2.3 %collective-permute-start.6 = (bf16[2048,128]{1,0:T(8,128)(2,1)S(1)}, bf16[2048,128]{1,0:T(8,128)(2,1)S(1)}, u32[]{:S(2)}, u32[]{:S(2)}) collective-permute-start(bf16[2048,128]{1,0:T(8,128)(2,1)S(1)} %get-tuple-element.10), channel_id=1, source_target_pairs={{0,0},{1,16},{2,1},{3,17},{4,4},{5,20},{6,5},{7,21},{8,8},{9,24},{... | collective-permute-start | bytes 1572872 | tf_op jit(solution)/shard_map/ppermute | solution.py:224
  113.9 5.3 %collective-permute-start.7 = (bf16[2048,128]{1,0:T(8,128)(2,1)S(1)}, bf16[2048,128]{1,0:T(8,128)(2,1)S(1)}, u32[]{:S(2)}, u32[]{:S(2)}) collective-permute-start(bf16[2048,128]{1,0:T(8,128)(2,1)S(1)} %get-tuple-element.9), channel_id=1, source_target_pairs={{0,1},{1,17},{2,0},{3,16},{4,5},{5,21},{6,4},{7,20},{8,9},{9,25},{... | collective-permute-start | bytes 1572872 | tf_op jit(solution)/shard_map/ppermute | solution.py:224
  119.3 4.4 %collective-permute-done.6.d0 = bf16[2048,128]{1,0:T(8,128)(2,1)S(1)} collective-permute-done((bf16[2048,128]{1,0:T(8,128)(2,1)S(1)}, bf16[2048,128]{1,0:T(8,128)(2,1)S(1)}, u32[]{:S(2)}, u32[]{:S(2)}) %collective-permute-start.6) | collective-permute-done | bytes 524320 | tf_op jit(solution)/shard_map/ppermute | solution.py:224
  123.6 1.9 collective-permute-start.8
  125.6 5.8 %collective-permute-done.7.d1 = bf16[2048,128]{1,0:T(8,128)(2,1)S(1)} collective-permute-done((bf16[2048,128]{1,0:T(8,128)(2,1)S(1)}, bf16[2048,128]{1,0:T(8,128)(2,1)S(1)}, u32[]{:S(2)}, u32[]{:S(2)}) %collective-permute-start.7) | collective-permute-done | bytes 524320 | tf_op jit(solution)/shard_map/ppermute | solution.py:224
  131.4 1.9 collective-permute-start.9
  133.3 1.9 collective-permute-done.9.e1
  135.2 0.8 copy-done.1
  136.0 1.0 copy-done.2
  137.0 2.7 %shard_map.94 = bf16[1536,128]{1,0:T(8,128)(2,1)} custom-call(s32[5]{0:T(128)S(1)} %stack.33.pos_ref, bf16[192,192]{1,0:T(8,128)(2,1)S(1)} %copy-done.4, bf16[4,384,512]{2,1,0:T(8,128)(2,1)S(1)} %all-to-all-done.1.acts, bf16[2048,128]{1,0:T(8,128)(2,1)S(1)} %collective-permute-done.6.d0, bf16[2048,128]{1,0:T(8,128)(2,1)S(1)} %collective-permute-done.7.d1, ...), custom_call_target="tpu_custom_call" | custom-call | flops 1000000000 | bytes 4000000 | tf_op jit(solution)/shard_map/pallas_call | solution.py:276
  139.7 27.5 %all-to-all-start.2 = ((bf16[128,3,4,128]{3,2,1,0:T(4,128)(2,1)}), bf16[128,3,4,128]{3,2,1,0:T(4,128)(2,1)S(1)}, u32[]{:S(2)}, u32[]{:S(2)}) async-start(bf16[128,3,4,128]{3,2,1,0:T(4,128)(2,1)} %bitcast.13), calls=%async_computation.2 | async-start | bytes 786432 | tf_op jit(solution)/shard_map/all_to_all | solution.py:284
  167.2 0.1 copy.10.ids_ref
  167.5 1.7 shard_map.91.scale_ref
  169.2 51.0 %all-to-all-done.2 = bf16[128,3,4,128]{3,2,1,0:T(4,128)(2,1)S(1)} async-done(((bf16[128,3,4,128]{3,2,1,0:T(4,128)(2,1)}), bf16[128,3,4,128]{3,2,1,0:T(4,128)(2,1)S(1)}, u32[]{:S(2)}, u32[]{:S(2)}) %all-to-all-start.2) | async-done | bytes 393248 | tf_op jit(solution)/shard_map/all_to_all | solution.py:284
  220.2 1.2 shard_map.95
  (26 shorter events, 0.4 us)
Async XLA Ops:
  2.7 8.3 %copy-start = (bf16[256,2048]{1,0:T(8,128)(2,1)S(1)}, bf16[256,2048]{1,0:T(8,128)(2,1)}, u32[]{:S(2)}) copy-start(bf16[256,2048]{1,0:T(8,128)(2,1)} %tok_ref.1) | copy-start | bytes 3145732
  2.7 8.3 %copy-start.5 = (s32[256,4]{0,1:T(4,128)S(1)}, s32[256,4]{0,1:T(4,128)}, u32[]{:S(2)}) copy-start(s32[256,4]{0,1:T(4,128)} %param.11) | copy-start | bytes 12292
  2.7 8.3 %copy-start.6 = (f32[2048]{0:T(1024)S(1)}, f32[2048]{0:T(1024)}, u32[]{:S(2)}) copy-start(f32[2048]{0:T(1024)} %param.10) | copy-start | bytes 24580
  2.7 79.1 %collective-permute-start.2 = (bf16[2,2048,128]{2,1,0:T(8,128)(2,1)}, bf16[2,2048,128]{2,1,0:T(8,128)(2,1)S(1)}, u32[]{:S(2)}, u32[]{:S(2)}) collective-permute-start(bf16[2,2048,128]{2,1,0:T(8,128)(2,1)} %pad_maximum_fusion), channel_id=1, source_target_pairs={{0,0},{1,16},{2,1},{3,17},{4,4},{5,20},{6,5},{7,21},{8,8},{9,24},{... | collective-permute-start | bytes 3145736 | tf_op jit(solution)/shard_map/ppermute | solution.py:224
  6.7 77.0 %collective-permute-start.3 = (bf16[2,2048,128]{2,1,0:T(8,128)(2,1)}, bf16[2,2048,128]{2,1,0:T(8,128)(2,1)}, u32[]{:S(2)}, u32[]{:S(2)}) collective-permute-start(bf16[2,2048,128]{2,1,0:T(8,128)(2,1)} %pad_maximum_fusion.1), channel_id=1, source_target_pairs={{0,1},{1,17},{2,0},{3,16},{4,5},{5,21},{6,4},{7,20},{8,9},{9,25},{... | collective-permute-start | bytes 3145736 | tf_op jit(solution)/shard_map/ppermute | solution.py:224
  12.6 27.3 %collective-permute-start = (bf16[96,1024]{1,0:T(8,128)(2,1)S(1)}, bf16[96,1024]{1,0:T(8,128)(2,1)S(1)}, u32[]{:S(2)}, u32[]{:S(2)}) collective-permute-start(bf16[96,1024]{1,0:T(8,128)(2,1)S(1)} %get-tuple-element.7), channel_id=1, source_target_pairs={{0,32},{1,65},{2,98},{3,131},{4,164},{5,197},{6,230},{7,263},{8,29... | collective-permute-start | bytes 589832 | tf_op jit(solution)/shard_map/ppermute | solution.py:224
  28.4 40.0 %collective-permute-start.1 = (bf16[96,1024]{1,0:T(8,128)(2,1)S(1)}, bf16[96,1024]{1,0:T(8,128)(2,1)S(1)}, u32[]{:S(2)}, u32[]{:S(2)}) collective-permute-start(bf16[96,1024]{1,0:T(8,128)(2,1)S(1)} %get-tuple-element.8), channel_id=1, source_target_pairs={{0,544},{1,577},{2,610},{3,643},{4,676},{5,709},{6,742},{7,775},{8... | collective-permute-start | bytes 589832 | tf_op jit(solution)/shard_map/ppermute | solution.py:224
  69.7 32.3 %copy-start.3 = (bf16[192,192]{1,0:T(8,128)(2,1)S(1)}, bf16[192,192]{1,0:T(8,128)(2,1)}, u32[]{:S(2)}) copy-start(bf16[192,192]{1,0:T(8,128)(2,1)} %constant.39.clone.perm_ref) | copy-start | bytes 221188
  69.7 32.3 %all-to-all-start = ((bf16[16,48,1024]{2,1,0:T(8,128)(2,1)}), bf16[16,48,1024]{2,1,0:T(8,128)(2,1)S(1)}, u32[]{:S(2)}, u32[]{:S(2)}) async-start(bf16[16,48,1024]{2,1,0:T(8,128)(2,1)} %bitcast.21), calls=%async_computation | async-start | bytes 3145728 | tf_op jit(solution)/shard_map/all_to_all | solution.py:264
  81.8 20.3 %collective-permute-start.4 = (bf16[2,2048,128]{2,1,0:T(8,128)(2,1)S(1)}, bf16[2,2048,128]{2,1,0:T(8,128)(2,1)}, u32[]{:S(2)}, u32[]{:S(2)}) collective-permute-start(bf16[2,2048,128]{2,1,0:T(8,128)(2,1)S(1)} %collective-permute-done.2.w0), channel_id=1, source_target_pairs={{0,16},{1,17},{2,18},{3,19},{4,20},{5,21},{6,22},{7,23},{8,24},{9,... | collective-permute-start | bytes 3145736 | tf_op jit(solution)/shard_map/ppermute | solution.py:224
  83.7 18.3 %collective-permute-start.5 = (bf16[2,2048,128]{2,1,0:T(8,128)(2,1)}, bf16[2,2048,128]{2,1,0:T(8,128)(2,1)}, u32[]{:S(2)}, u32[]{:S(2)}) collective-permute-start(bf16[2,2048,128]{2,1,0:T(8,128)(2,1)} %collective-permute-done.3.w1), channel_id=1, source_target_pairs={{0,16},{1,17},{2,18},{3,19},{4,20},{5,21},{6,22},{7,23},{8,24},{9,... | collective-permute-start | bytes 3145736 | tf_op jit(solution)/shard_map/ppermute | solution.py:224
  107.4 4.1 %copy-start.7 = (bf16[2,2048,128]{2,1,0:T(8,128)(2,1)S(1)}, bf16[2,2048,128]{2,1,0:T(8,128)(2,1)}, u32[]{:S(2)}) copy-start(bf16[2,2048,128]{2,1,0:T(8,128)(2,1)} %param.15) | copy-start | bytes 3145732
  107.4 28.5 %all-to-all-start.1 = ((bf16[4,384,512]{2,1,0:T(8,128)(2,1)}), bf16[4,384,512]{2,1,0:T(8,128)(2,1)S(1)}, u32[]{:S(2)}, u32[]{:S(2)}) async-start(bf16[4,384,512]{2,1,0:T(8,128)(2,1)} %shard_map.93), calls=%async_computation.1 | async-start | bytes 3145728 | tf_op jit(solution)/shard_map/all_to_all | solution.py:275
  111.5 24.5 %copy-start.4 = (bf16[192,192]{1,0:T(8,128)(2,1)S(1)}, bf16[192,192]{1,0:T(8,128)(2,1)}, u32[]{:S(2)}) copy-start(bf16[192,192]{1,0:T(8,128)(2,1)} %constant.40.clone.perm_ref) | copy-start | bytes 221188
  111.5 55.8 %copy-start.8 = (f32[256,4]{0,1:T(4,128)S(1)}, f32[256,4]{0,1:T(4,128)}, u32[]{:S(2)}) copy-start(f32[256,4]{0,1:T(4,128)} %param.12) | copy-start | bytes 12292
  111.6 12.1 %collective-permute-start.6 = (bf16[2048,128]{1,0:T(8,128)(2,1)S(1)}, bf16[2048,128]{1,0:T(8,128)(2,1)S(1)}, u32[]{:S(2)}, u32[]{:S(2)}) collective-permute-start(bf16[2048,128]{1,0:T(8,128)(2,1)S(1)} %get-tuple-element.10), channel_id=1, source_target_pairs={{0,0},{1,16},{2,1},{3,17},{4,4},{5,20},{6,5},{7,21},{8,8},{9,24},{... | collective-permute-start | bytes 1572872 | tf_op jit(solution)/shard_map/ppermute | solution.py:224
  113.9 17.5 %collective-permute-start.7 = (bf16[2048,128]{1,0:T(8,128)(2,1)S(1)}, bf16[2048,128]{1,0:T(8,128)(2,1)S(1)}, u32[]{:S(2)}, u32[]{:S(2)}) collective-permute-start(bf16[2048,128]{1,0:T(8,128)(2,1)S(1)} %get-tuple-element.9), channel_id=1, source_target_pairs={{0,1},{1,17},{2,0},{3,16},{4,5},{5,21},{6,4},{7,20},{8,9},{9,25},{... | collective-permute-start | bytes 1572872 | tf_op jit(solution)/shard_map/ppermute | solution.py:224
  123.6 9.7 %collective-permute-start.8 = (bf16[2048,128]{1,0:T(8,128)(2,1)S(1)}, bf16[2048,128]{1,0:T(8,128)(2,1)S(1)}, u32[]{:S(2)}, u32[]{:S(2)}) collective-permute-start(bf16[2048,128]{1,0:T(8,128)(2,1)S(1)} %collective-permute-done.6.d0), channel_id=1, source_target_pairs={{0,16},{1,17},{2,18},{3,19},{4,20},{5,21},{6,22},{7,23},{8,24},{9,... | collective-permute-start | bytes 1572872 | tf_op jit(solution)/shard_map/ppermute | solution.py:224
  131.4 3.8 %collective-permute-start.9 = (bf16[2048,128]{1,0:T(8,128)(2,1)S(1)}, bf16[2048,128]{1,0:T(8,128)(2,1)S(1)}, u32[]{:S(2)}, u32[]{:S(2)}) collective-permute-start(bf16[2048,128]{1,0:T(8,128)(2,1)S(1)} %collective-permute-done.7.d1), channel_id=1, source_target_pairs={{0,16},{1,17},{2,18},{3,19},{4,20},{5,21},{6,22},{7,23},{8,24},{9,... | collective-permute-start | bytes 1572872 | tf_op jit(solution)/shard_map/ppermute | solution.py:224
  135.2 0.8 copy-start.1
  136.0 1.0 copy-start.2
  139.7 80.5 %all-to-all-start.2 = ((bf16[128,3,4,128]{3,2,1,0:T(4,128)(2,1)}), bf16[128,3,4,128]{3,2,1,0:T(4,128)(2,1)S(1)}, u32[]{:S(2)}, u32[]{:S(2)}) async-start(bf16[128,3,4,128]{3,2,1,0:T(4,128)(2,1)} %bitcast.13), calls=%async_computation.2 | async-start | bytes 786432 | tf_op jit(solution)/shard_map/all_to_all | solution.py:284

commit v2 on v1

--- a/solution.py
+++ b/solution.py
@@ -18,7 +18,7 @@
 ROWS = CHIPS * CAP
 UNIT = 2 * CAP
 SLAB = SIDE * CAP
-HALF = 1024
+HALF = 256
 LANES = 128
 BLOCK = SIDE * LANES
 BF = jnp.bfloat16
@@ -39,21 +39,22 @@
     return jnp.where(mask, 1.0, 0.0).astype(BF)
 
 
-def prep_kernel(pos_ref, tok_ref, gain_ref, ids_ref, out0_ref, out1_ref):
+def prep_kernel(pos_ref, tok_ref, gain_ref, ids_ref, out_ref):
+    x, y = pos_ref[1], pos_ref[3]
     values = tok_ref[...].astype(F32)
     row_mean = jnp.mean(values, axis=1, keepdims=True)
     centred = values - row_mean
     row_var = jnp.mean(centred * centred, axis=1, keepdims=True)
-    normed = (centred * lax.rsqrt(row_var + norm_eps) * gain_ref[...]).astype(BF)
-    shape = (2 * SIDE * UNIT, TOK)
+    cols = pl.ds(pl.multiple_of(y * BLOCK, BLOCK), BLOCK)
+    own = tok_ref[:, cols].astype(F32) - row_mean
+    normed = (own * lax.rsqrt(row_var + norm_eps) * gain_ref[:, cols]).astype(BF)
+    shape = (CHIPS * UNIT, TOK)
     r = iota(shape, 0)
-    second = r >= SIDE * UNIT
-    rest = jnp.where(second, r - SIDE * UNIT, r)
-    q = (rest * 2731) >> 16
-    rest = rest - q * UNIT
+    chip = (r * 2731) >> 16
+    rest = r - chip * UNIT
     half = rest >= CAP
     slot = jnp.where(half, rest - CAP, rest)
-    name = jnp.where(second, pos_ref[4], pos_ref[3]) * SIDE + q
+    name = chip * SIDE + x
     named = name == ids_ref[0:1, :]
     for k in range(1, 4):
         named = named | (name == ids_ref[k : k + 1, :])
@@ -61,10 +62,7 @@
     rank = jnp.dot(as_bf(named), before, preferred_element_type=F32)
     placed = as_bf(named & (rank == slot.astype(F32)))
     wide = jnp.dot(placed, normed, preferred_element_type=F32)
-    upper = half[:, :1]
-    out = jnp.where(upper, wide[:, HALF:], wide[:, :HALF]).astype(BF)
-    out0_ref[...] = out[: SIDE * UNIT]
-    out1_ref[...] = out[SIDE * UNIT :]
+    out_ref[...] = jnp.where(half[:, :1], wide[:, HALF:], wide[:, :HALF]).astype(BF)
 
 
 def scale_kernel(ids_ref, weight_ref, out_ref):
@@ -97,7 +95,7 @@
 
 
 def unpack_matrix():
-    n = GROUP * 2 * UNIT
+    n = 2 * GROUP * UNIT
     q = np.arange(n)
     half, unit, slot = q // (n // 2), q % (n // 2) // CAP, q % CAP
     m = np.zeros((n, n), np.float32)
@@ -116,14 +114,17 @@
 
 def gate_up_kernel(pos_ref, perm_ref, raw_ref, w0, w1, v0, v1, act_ref, xs):
     core, x = pos_ref[0], pos_ref[1]
-    n = GROUP * 2 * UNIT
-    for g in range(PLANE // GROUP):
-        part = jnp.dot(
-            perm_ref[...], raw_ref[g * n : (g + 1) * n, :], preferred_element_type=F32
-        ).astype(BF)
-        rows = slice(g * n // 2, (g + 1) * n // 2)
-        xs[rows, :HALF] = part[: n // 2]
-        xs[rows, HALF:] = part[n // 2 :]
+    n, m = 2 * GROUP * UNIT, 2 * GROUP * CAP
+    for y in range(SIDE):
+        for g in range(CHIPS // (2 * GROUP)):
+            part = jnp.dot(
+                perm_ref[...],
+                raw_ref[y, g * n : (g + 1) * n, :],
+                preferred_element_type=F32,
+            ).astype(BF)
+            for h in range(2):
+                cols = slice((2 * y + h) * HALF, (2 * y + h + 1) * HALF)
+                xs[g * m : (g + 1) * m, cols] = part[h * m : (h + 1) * m]
     for k, (own, w) in enumerate(((1, w0), (1, w1), (0, v0), (0, v1))):
         both = jnp.concatenate([w[0], w[1]], axis=1)
         pre = jnp.dot(xs[...], both, preferred_element_type=F32)
@@ -135,7 +136,7 @@
 
 
 def down_kernel(pos_ref, perm_ref, acts, d0, d1, e0, e1, out_ref, res):
-    core, x, z = pos_ref[0], pos_ref[1], pos_ref[2]
+    core, x = pos_ref[0], pos_ref[1]
     for own, pair in ((1, (d0, d1)), (0, (e0, e1))):
         total = jnp.zeros((ROWS, 2 * LANES), F32)
         for i in range(SIDE):
@@ -147,20 +148,15 @@
             col = 2 * ((x + k) % 2) + (core if own else 1 - core)
             cols = pl.ds(pl.multiple_of(col * LANES, LANES), LANES)
             res[:, cols] = out[:, k * LANES : (k + 1) * LANES]
-    sign = 1 - 2 * core
     for g in range(CHIPS // GROUP):
         rows = slice(g * SLAB, (g + 1) * SLAB)
         part = jnp.concatenate(
             [res[rows, cb * LANES : (cb + 1) * LANES] for cb in range(SIDE)], axis=0
         )
-        part = jnp.dot(perm_ref[...], part, preferred_element_type=F32).astype(BF)
-        for i in range(GROUP):
-            t, m = divmod(g * GROUP + i, 2)
-            shift = sign * (-(15 - t) if m else t + 1)
-            source = (z - shift + 2 * CHIPS) % CHIPS
-            out_ref[pl.ds(pl.multiple_of(source * SLAB, SLAB), SLAB), :] = part[
-                i * SLAB : (i + 1) * SLAB
-            ]
+        n = GROUP * SLAB
+        out_ref[g * n : (g + 1) * n, :] = jnp.dot(
+            perm_ref[...], part, preferred_element_type=F32
+        ).astype(BF)
 
 
 def call(kernel, out_shape, n_in, flops, nbytes, scratch=(), scalars=True):
@@ -191,18 +187,6 @@
     return (2 * (z % CHIPS) + c) * PLANE + SIDE * y + x
 
 
-def shift_of(m, c, t):
-    s = -(15 - t) if m else t + 1
-    return s if c == 0 else -s
-
-
-def z_pairs(m):
-    return [
-        (at(z, c, y, x), at(z + shift_of(m, c, SIDE * y + x), c, y, x))
-        for z, c, y, x in devices()
-    ]
-
-
 def weight_pairs(k):
     return [
         (at(z, c, y, x), at(z, x % 2, y, 2 * c + (x // 2 + k) % 2))
@@ -211,6 +195,7 @@
 
 
 SIBLING = [(at(z, c, y, x), at(z, 1 - c, y, x)) for z, c, y, x in devices()]
+CORE_GROUPS = [[2 * z + c for z in range(CHIPS)] for c in range(2)]
 Y_GROUPS = [[SIDE * y + x for y in range(SIDE)] for x in range(SIDE)]
 BACK_GROUPS = [
     [at(z, c, y, x) for z in range(CHIPS) for x in range(SIDE)]
@@ -224,19 +209,18 @@
     return lax.ppermute(a, BOTH, pairs)
 
 
+def exchange(a, axes, groups):
+    return lax.all_to_all(a, axes, 0, 0, tiled=True, axis_index_groups=groups)
+
+
 def per_device(tokens, norm_gain, route_ids, route_weights, w_gate, w_up, w_down):
     tp, ep = lax.axis_index("tp"), lax.axis_index("ep")
     x, z, core = tp & 3, ep >> 1, ep & 1
-    sign = 1 - 2 * core
-    pos = jnp.stack(
-        [core, x, z, (z + sign * (tp + 1)) & 31, (z - sign * (15 - tp)) & 31]
-    ).astype(jnp.int32)
-
-    message = jax.ShapeDtypeStruct((SIDE * UNIT, HALF), BF)
-    out0, out1 = call(prep_kernel, (message, message), 4, 10**8, 2 * 10**6)(
-        pos, tokens, norm_gain.reshape(1, -1), route_ids.T
-    )
-    got = [permute(out, z_pairs(m)) for m, out in enumerate((out0, out1))]
+    pos = jnp.stack([core, x, z, tp >> 2]).astype(jnp.int32)
+    outgoing = call(
+        prep_kernel, jax.ShapeDtypeStruct((CHIPS * UNIT, HALF), BF), 4, 10**8, 2 * 10**6
+    )(pos, tokens, norm_gain.reshape(1, -1), route_ids.T)
+    raw = exchange(outgoing.reshape(CHIPS, UNIT, HALF), "ep", CORE_GROUPS)
 
     def pick(w, i):
         return lax.dynamic_index_in_dim(w, i, 0, keepdims=False)
@@ -259,20 +243,19 @@
         scalars=False,
     )(route_ids, route_weights)
 
-    units = jnp.concatenate([g.reshape(SIDE, UNIT, HALF) for g in got], axis=1)
-    units = jnp.broadcast_to(units[None], (SIDE, SIDE, 2 * UNIT, HALF))
-    raw = lax.all_to_all(
-        units.reshape(PLANE, 2 * UNIT, HALF), "tp", 0, 0, tiled=True
-    ).reshape(2 * ROWS, HALF)
+    raw = jnp.broadcast_to(
+        raw.reshape(1, CHIPS * UNIT, HALF), (SIDE, CHIPS * UNIT, HALF)
+    )
+    raw = exchange(raw, "tp", Y_GROUPS)
     act = call(
         gate_up_kernel,
         jax.ShapeDtypeStruct((SIDE, ROWS, BLOCK), BF),
         7,
         2 * 10**9,
         6 * 10**6,
-        [pltpu.VMEM((ROWS, 2 * HALF), BF)],
+        [pltpu.VMEM((ROWS, SIDE * BLOCK), BF)],
     )(pos, jnp.asarray(unpack_matrix(), BF), raw, *gu_blocks)
-    acts = lax.all_to_all(act, "tp", 0, 0, tiled=True, axis_index_groups=Y_GROUPS)
+    acts = exchange(act, "tp", Y_GROUPS)
     result = call(
         down_kernel,
         jax.ShapeDtypeStruct((4 * ROWS, LANES), BF),
@@ -281,13 +264,8 @@
         4 * 10**6,
         [pltpu.VMEM((ROWS, BLOCK), BF)],
     )(pos, jnp.asarray(pack_matrix(), BF), acts, *wd_blocks)
-    returned = lax.all_to_all(
-        result.reshape(4 * CHIPS, 3, 4, LANES),
-        BOTH,
-        0,
-        0,
-        tiled=True,
-        axis_index_groups=BACK_GROUPS,
+    returned = exchange(
+        result.reshape(4 * CHIPS, 3, 4, LANES), BOTH, BACK_GROUPS
     ).reshape(4 * ROWS, LANES)
     return call(
         combine_kernel,

time: 222 us -> 214 us (0.964)
  starting transfers between devices: 91.4 us -> 70.2 us
  waiting for transfers between devices: 110 us -> 117 us
  local copies, waits for them, and re-layouts: 5.31 us -> 10.6 us
    all_to_all x3 -> x4, waiting for transfers between devices: 66.9 us -> 105 us  [exchange(): return lax.all_to_all(a, axes, 0, 0, tiled=True, axis_index_groups=groups)]
    ppermute x10 -> x8, waiting for transfers between devices: 42.9 us -> 12.5 us  [permute(): return lax.ppermute(a, BOTH, pairs)]
    ppermute x10 -> x8, starting transfers between devices: 47.9 us -> 22.2 us  [permute(): return lax.ppermute(a, BOTH, pairs)]
    unnamed x20 -> x34, local copies, waits for them, and re-layouts: 2.12 us -> 9.12 us
    all_to_all x3 -> x4, starting transfers between devices: 43.6 us -> 48 us  [exchange(): return lax.all_to_all(a, axes, 0, 0, tiled=True, axis_index_groups=groups)]
  transfers between devices with their start and end apart: 13 -> 12, of which waited for: 7 -> 8; matrix products, arithmetic and copies ran while one was open for 1% -> 2% of each run, Pallas kernels for 1% -> 1%
where the time goes in v2:
time: 214 us; the launch traced here: 213 us
  waiting for transfers between devices  117 us (55%)
  starting transfers between devices  70.2 us (33%)
  Pallas kernels  12.8 us (6%)
  local copies, waits for them, and re-layouts  10.6 us (5%)
  other arithmetic  2.2 us (1%)
    all_to_all x4, waiting for transfers between devices, exchange(): return lax.all_to_all(a, axes, 0, 0, tiled=True, axis_index_groups=groups)  105 us
    all_to_all x4, starting transfers between devices, exchange(): return lax.all_to_all(a, axes, 0, 0, tiled=True, axis_index_groups=groups)  48 us
    ppermute x8, starting transfers between devices, permute(): return lax.ppermute(a, BOTH, pairs)  22.2 us
    ppermute x8, waiting for transfers between devices, permute(): return lax.ppermute(a, BOTH, pairs)  12.5 us
    unnamed x34, local copies, waits for them, and re-layouts  9.12 us
    pallas_call x1, Pallas kernels, per_device(): call(gate_up_kernel, jax.ShapeDtypeStruct((SIDE, ROWS, BLOCK), BF), 7, 2...  4.79 us
  transfers between devices with their start and end apart: 12, of which 8 were waited for; matrix products, arithmetic and copies ran while one was open for 2% of the time, Pallas kernels for 1%

profile of v2, /device:TPU:14, one launch (start us, length us, event | category | flops | bytes accessed | tf_op | source)
XLA Modules:
  0.0 213.5 jit_solution(2297872952960901971)
XLA Ops:
  0.1 1.2 copy-done
  2.7 2.5 %shard_map.92 = bf16[768,256]{1,0:T(8,128)(2,1)} custom-call(s32[4]{0:T(128)S(1)} %pad_add_fusion.pos_ref, bf16[256,2048]{1,0:T(8,128)(2,1)S(1)} %copy-done, f32[1,2048]{1,0:T(1,128)S(1)} %bitcast.16, s32[4,256]{1,0:T(4,128)S(1)} %bitcast.15), custom_call_target="tpu_custom_call" | custom-call | flops 100000000 | bytes 2000000 | tf_op jit(solution)/shard_map/pallas_call | solution.py:220
  5.2 28.7 %all-to-all-start = ((bf16[32,24,256]{2,1,0:T(8,128)(2,1)}), bf16[32,24,256]{2,1,0:T(8,128)(2,1)S(1)}, u32[]{:S(2)}, u32[]{:S(2)}) async-start(bf16[32,24,256]{2,1,0:T(8,128)(2,1)} %bitcast.6), calls=%async_computation | async-start | bytes 786432 | tf_op jit(solution)/shard_map/all_to_all | solution.py:213
  34.1 1.1 pad_maximum_fusion
  35.2 2.5 %collective-permute-start = (bf16[2,2048,128]{2,1,0:T(8,128)(2,1)}, bf16[2,2048,128]{2,1,0:T(8,128)(2,1)S(1)}, u32[]{:S(2)}, u32[]{:S(2)}) collective-permute-start(bf16[2,2048,128]{2,1,0:T(8,128)(2,1)} %pad_maximum_fusion), channel_id=1, source_target_pairs={{0,0},{1,16},{2,1},{3,17},{4,4},{5,20},{6,5},{7,21},{8,8},{9,24},{... | collective-permute-start | bytes 3145736 | tf_op jit(solution)/shard_map/ppermute | solution.py:209
  37.7 1.1 pad_maximum_fusion.1
  38.7 4.6 %collective-permute-start.1 = (bf16[2,2048,128]{2,1,0:T(8,128)(2,1)}, bf16[2,2048,128]{2,1,0:T(8,128)(2,1)}, u32[]{:S(2)}, u32[]{:S(2)}) collective-permute-start(bf16[2,2048,128]{2,1,0:T(8,128)(2,1)} %pad_maximum_fusion.1), channel_id=1, source_target_pairs={{0,1},{1,17},{2,0},{3,16},{4,5},{5,21},{6,4},{7,20},{8,9},{9,25},{... | collective-permute-start | bytes 3145736 | tf_op jit(solution)/shard_map/ppermute | solution.py:209
  43.3 44.4 %all-to-all-done = bf16[32,24,256]{2,1,0:T(8,128)(2,1)S(1)} async-done(((bf16[32,24,256]{2,1,0:T(8,128)(2,1)}), bf16[32,24,256]{2,1,0:T(8,128)(2,1)S(1)}, u32[]{:S(2)}, u32[]{:S(2)}) %all-to-all-start) | async-done | bytes 393248 | tf_op jit(solution)/shard_map/all_to_all | solution.py:213
  87.7 1.3 broadcast_in_dim.8
  89.0 5.0 %all-to-all-start.1 = ((bf16[4,768,256]{2,1,0:T(8,128)(2,1)}), bf16[4,768,256]{2,1,0:T(8,128)(2,1)S(1)}, u32[]{:S(2)}, u32[]{:S(2)}) async-start(bf16[4,768,256]{2,1,0:T(8,128)(2,1)} %broadcast_in_dim.8), calls=%async_computation.1 | async-start | bytes 3145728 | tf_op jit(solution)/shard_map/all_to_all | solution.py:213
  94.0 1.9 collective-permute-start.2
  95.9 2.4 %collective-permute-start.3 = (bf16[2,2048,128]{2,1,0:T(8,128)(2,1)}, bf16[2,2048,128]{2,1,0:T(8,128)(2,1)S(1)}, u32[]{:S(2)}, u32[]{:S(2)}) collective-permute-start(bf16[2,2048,128]{2,1,0:T(8,128)(2,1)} %collective-permute-done.1.w1), channel_id=1, source_target_pairs={{0,16},{1,17},{2,18},{3,19},{4,20},{5,21},{6,22},{7,23},{8,24},{9,... | collective-permute-start | bytes 3145736 | tf_op jit(solution)/shard_map/ppermute | solution.py:209
  98.6 1.0 copy-done.1
  99.5 1.3 collective-permute-done.3.v1
  101.8 9.4 %all-to-all-done.1.raw_ref = bf16[4,768,256]{2,1,0:T(8,128)(2,1)S(1)} async-done(((bf16[4,768,256]{2,1,0:T(8,128)(2,1)}), bf16[4,768,256]{2,1,0:T(8,128)(2,1)S(1)}, u32[]{:S(2)}, u32[]{:S(2)}) %all-to-all-start.1) | async-done | bytes 1572896 | tf_op jit(solution)/shard_map/all_to_all | solution.py:213
  111.2 1.2 copy-done.2
  112.5 1.2 copy-done.4
  113.7 4.8 %shard_map.93 = bf16[4,384,512]{2,1,0:T(8,128)(2,1)} custom-call(s32[4]{0:T(128)S(1)} %pad_add_fusion.pos_ref, bf16[192,192]{1,0:T(8,128)(2,1)S(1)} %copy-done.7, bf16[4,768,256]{2,1,0:T(8,128)(2,1)S(1)} %all-to-all-done.1.raw_ref, bf16[2,2048,128]{2,1,0:T(8,128)(2,1)S(1)} %collective-permute-done.w0, bf16[2,2048,128]{2,1,0:T(8,128)(2,1)} %collective-permute-done.1.w1, ...), custom_call_target="tpu_custom_call" | custom-call | flops 2000000000 | bytes 6000000 | tf_op jit(solution)/shard_map/pallas_call | solution.py:250
  118.5 5.1 %all-to-all-start.2 = ((bf16[4,384,512]{2,1,0:T(8,128)(2,1)}), bf16[4,384,512]{2,1,0:T(8,128)(2,1)S(1)}, u32[]{:S(2)}, u32[]{:S(2)}) async-start(bf16[4,384,512]{2,1,0:T(8,128)(2,1)} %shard_map.93), calls=%async_computation.2 | async-start | bytes 3145728 | tf_op jit(solution)/shard_map/all_to_all | solution.py:213
  123.7 1.9 collective-permute-start.4
  125.6 5.1 %collective-permute-start.5 = (bf16[2048,128]{1,0:T(8,128)(2,1)S(1)}, bf16[2048,128]{1,0:T(8,128)(2,1)S(1)}, u32[]{:S(2)}, u32[]{:S(2)}) collective-permute-start(bf16[2048,128]{1,0:T(8,128)(2,1)S(1)} %get-tuple-element.5), channel_id=1, source_target_pairs={{0,1},{1,17},{2,0},{3,16},{4,5},{5,21},{6,4},{7,20},{8,9},{9,25},{... | collective-permute-start | bytes 1572872 | tf_op jit(solution)/shard_map/ppermute | solution.py:209
  130.8 7.2 %collective-permute-done.4.d0 = bf16[2048,128]{1,0:T(8,128)(2,1)S(1)} collective-permute-done((bf16[2048,128]{1,0:T(8,128)(2,1)S(1)}, bf16[2048,128]{1,0:T(8,128)(2,1)S(1)}, u32[]{:S(2)}, u32[]{:S(2)}) %collective-permute-start.4) | collective-permute-done | bytes 524320 | tf_op jit(solution)/shard_map/ppermute | solution.py:209
  138.0 1.9 collective-permute-start.6
  139.9 2.0 collective-permute-done.5.d1
  141.8 1.9 collective-permute-start.7
  143.8 1.9 collective-permute-done.7.e1
  146.4 1.0 copy-done.6
  147.5 2.7 %shard_map.94 = bf16[1536,128]{1,0:T(8,128)(2,1)} custom-call(s32[4]{0:T(128)S(1)} %pad_add_fusion.pos_ref, bf16[192,192]{1,0:T(8,128)(2,1)S(1)} %copy-done.8, bf16[4,384,512]{2,1,0:T(8,128)(2,1)S(1)} %all-to-all-done.2.acts, bf16[2048,128]{1,0:T(8,128)(2,1)S(1)} %collective-permute-done.4.d0, bf16[2048,128]{1,0:T(8,128)(2,1)S(1)} %collective-permute-done.5.d1, ...), custom_call_target="tpu_custom_call" | custom-call | flops 1000000000 | bytes 4000000 | tf_op jit(solution)/shard_map/pallas_call | solution.py:259
  150.1 9.1 %all-to-all-start.3 = ((bf16[128,3,4,128]{3,2,1,0:T(4,128)(2,1)}), bf16[128,3,4,128]{3,2,1,0:T(4,128)(2,1)S(1)}, u32[]{:S(2)}, u32[]{:S(2)}) async-start(bf16[128,3,4,128]{3,2,1,0:T(4,128)(2,1)} %bitcast.10), calls=%async_computation.3 | async-start | bytes 786432 | tf_op jit(solution)/shard_map/all_to_all | solution.py:213
  159.6 1.7 shard_map.91.scale_ref
  161.3 51.0 %all-to-all-done.3 = bf16[128,3,4,128]{3,2,1,0:T(4,128)(2,1)S(1)} async-done(((bf16[128,3,4,128]{3,2,1,0:T(4,128)(2,1)}), bf16[128,3,4,128]{3,2,1,0:T(4,128)(2,1)S(1)}, u32[]{:S(2)}, u32[]{:S(2)}) %all-to-all-start.3) | async-done | bytes 393248 | tf_op jit(solution)/shard_map/all_to_all | solution.py:213
  212.3 1.2 shard_map.95
  (37 shorter events, 3.9 us)
Async XLA Ops:
  0.1 1.2 copy-start
  1.3 0.7 copy-start.9
  2.0 0.7 copy-start.11
  2.7 31.3 %copy-start.12 = (bf16[2,2048,128]{2,1,0:T(8,128)(2,1)S(1)}, bf16[2,2048,128]{2,1,0:T(8,128)(2,1)}, u32[]{:S(2)}) copy-start(bf16[2,2048,128]{2,1,0:T(8,128)(2,1)} %param.14) | copy-start | bytes 3145732
  2.7 31.3 %copy-start.13 = (bf16[2,2048,128]{2,1,0:T(8,128)(2,1)S(1)}, bf16[2,2048,128]{2,1,0:T(8,128)(2,1)}, u32[]{:S(2)}) copy-start(bf16[2,2048,128]{2,1,0:T(8,128)(2,1)} %param.13) | copy-start | bytes 3145732
  5.2 82.5 %all-to-all-start = ((bf16[32,24,256]{2,1,0:T(8,128)(2,1)}), bf16[32,24,256]{2,1,0:T(8,128)(2,1)S(1)}, u32[]{:S(2)}, u32[]{:S(2)}) async-start(bf16[32,24,256]{2,1,0:T(8,128)(2,1)} %bitcast.6), calls=%async_computation | async-start | bytes 786432 | tf_op jit(solution)/shard_map/all_to_all | solution.py:213
  35.2 58.8 %collective-permute-start = (bf16[2,2048,128]{2,1,0:T(8,128)(2,1)}, bf16[2,2048,128]{2,1,0:T(8,128)(2,1)S(1)}, u32[]{:S(2)}, u32[]{:S(2)}) collective-permute-start(bf16[2,2048,128]{2,1,0:T(8,128)(2,1)} %pad_maximum_fusion), channel_id=1, source_target_pairs={{0,0},{1,16},{2,1},{3,17},{4,4},{5,20},{6,5},{7,21},{8,8},{9,24},{... | collective-permute-start | bytes 3145736 | tf_op jit(solution)/shard_map/ppermute | solution.py:209
  38.7 57.2 %collective-permute-start.1 = (bf16[2,2048,128]{2,1,0:T(8,128)(2,1)}, bf16[2,2048,128]{2,1,0:T(8,128)(2,1)}, u32[]{:S(2)}, u32[]{:S(2)}) collective-permute-start(bf16[2,2048,128]{2,1,0:T(8,128)(2,1)} %pad_maximum_fusion.1), channel_id=1, source_target_pairs={{0,1},{1,17},{2,0},{3,16},{4,5},{5,21},{6,4},{7,20},{8,9},{9,25},{... | collective-permute-start | bytes 3145736 | tf_op jit(solution)/shard_map/ppermute | solution.py:209
  89.0 22.3 %copy-start.7 = (bf16[192,192]{1,0:T(8,128)(2,1)S(1)}, bf16[192,192]{1,0:T(8,128)(2,1)}, u32[]{:S(2)}) copy-start(bf16[192,192]{1,0:T(8,128)(2,1)} %constant.35.clone.perm_ref) | copy-start | bytes 221188
  89.0 22.2 %all-to-all-start.1 = ((bf16[4,768,256]{2,1,0:T(8,128)(2,1)}), bf16[4,768,256]{2,1,0:T(8,128)(2,1)S(1)}, u32[]{:S(2)}, u32[]{:S(2)}) async-start(bf16[4,768,256]{2,1,0:T(8,128)(2,1)} %broadcast_in_dim.8), calls=%async_computation.1 | async-start | bytes 3145728 | tf_op jit(solution)/shard_map/all_to_all | solution.py:213
  94.0 4.5 %collective-permute-start.2 = (bf16[2,2048,128]{2,1,0:T(8,128)(2,1)S(1)}, bf16[2,2048,128]{2,1,0:T(8,128)(2,1)S(1)}, u32[]{:S(2)}, u32[]{:S(2)}) collective-permute-start(bf16[2,2048,128]{2,1,0:T(8,128)(2,1)S(1)} %collective-permute-done.w0), channel_id=1, source_target_pairs={{0,16},{1,17},{2,18},{3,19},{4,20},{5,21},{6,22},{7,23},{8,24},{9,... | collective-permute-start | bytes 3145736 | tf_op jit(solution)/shard_map/ppermute | solution.py:209
  95.9 4.9 %collective-permute-start.3 = (bf16[2,2048,128]{2,1,0:T(8,128)(2,1)}, bf16[2,2048,128]{2,1,0:T(8,128)(2,1)S(1)}, u32[]{:S(2)}, u32[]{:S(2)}) collective-permute-start(bf16[2,2048,128]{2,1,0:T(8,128)(2,1)} %collective-permute-done.1.w1), channel_id=1, source_target_pairs={{0,16},{1,17},{2,18},{3,19},{4,20},{5,21},{6,22},{7,23},{8,24},{9,... | collective-permute-start | bytes 3145736 | tf_op jit(solution)/shard_map/ppermute | solution.py:209
  98.6 1.0 copy-start.1
  100.8 1.0 copy-start.3
  111.2 1.2 copy-start.2
  112.5 1.2 copy-start.4
  118.5 5.1 %copy-start.14 = (bf16[2,2048,128]{2,1,0:T(8,128)(2,1)S(1)}, bf16[2,2048,128]{2,1,0:T(8,128)(2,1)}, u32[]{:S(2)}) copy-start(bf16[2,2048,128]{2,1,0:T(8,128)(2,1)} %param.15) | copy-start | bytes 3145732
  118.5 28.0 %all-to-all-start.2 = ((bf16[4,384,512]{2,1,0:T(8,128)(2,1)}), bf16[4,384,512]{2,1,0:T(8,128)(2,1)S(1)}, u32[]{:S(2)}, u32[]{:S(2)}) async-start(bf16[4,384,512]{2,1,0:T(8,128)(2,1)} %shard_map.93), calls=%async_computation.2 | async-start | bytes 3145728 | tf_op jit(solution)/shard_map/all_to_all | solution.py:213
  123.6 22.8 %copy-start.8 = (bf16[192,192]{1,0:T(8,128)(2,1)S(1)}, bf16[192,192]{1,0:T(8,128)(2,1)}, u32[]{:S(2)}) copy-start(bf16[192,192]{1,0:T(8,128)(2,1)} %constant.36.clone.perm_ref) | copy-start | bytes 221188
  123.6 35.7 %copy-start.10 = (s32[256,4]{0,1:T(4,128)S(1)}, s32[256,4]{0,1:T(4,128)}, u32[]{:S(2)}) copy-start(s32[256,4]{0,1:T(4,128)} %param.11) | copy-start | bytes 12292
  123.6 35.8 %copy-start.15 = (f32[256,4]{0,1:T(4,128)S(1)}, f32[256,4]{0,1:T(4,128)}, u32[]{:S(2)}) copy-start(f32[256,4]{0,1:T(4,128)} %param.12) | copy-start | bytes 12292
  123.7 14.3 %collective-permute-start.4 = (bf16[2048,128]{1,0:T(8,128)(2,1)S(1)}, bf16[2048,128]{1,0:T(8,128)(2,1)S(1)}, u32[]{:S(2)}, u32[]{:S(2)}) collective-permute-start(bf16[2048,128]{1,0:T(8,128)(2,1)S(1)} %get-tuple-element.6), channel_id=1, source_target_pairs={{0,0},{1,16},{2,1},{3,17},{4,4},{5,20},{6,5},{7,21},{8,8},{9,24},{... | collective-permute-start | bytes 1572872 | tf_op jit(solution)/shard_map/ppermute | solution.py:209
  125.6 16.2 %collective-permute-start.5 = (bf16[2048,128]{1,0:T(8,128)(2,1)S(1)}, bf16[2048,128]{1,0:T(8,128)(2,1)S(1)}, u32[]{:S(2)}, u32[]{:S(2)}) collective-permute-start(bf16[2048,128]{1,0:T(8,128)(2,1)S(1)} %get-tuple-element.5), channel_id=1, source_target_pairs={{0,1},{1,17},{2,0},{3,16},{4,5},{5,21},{6,4},{7,20},{8,9},{9,25},{... | collective-permute-start | bytes 1572872 | tf_op jit(solution)/shard_map/ppermute | solution.py:209
  138.0 5.8 %collective-permute-start.6 = (bf16[2048,128]{1,0:T(8,128)(2,1)S(1)}, bf16[2048,128]{1,0:T(8,128)(2,1)S(1)}, u32[]{:S(2)}, u32[]{:S(2)}) collective-permute-start(bf16[2048,128]{1,0:T(8,128)(2,1)S(1)} %collective-permute-done.4.d0), channel_id=1, source_target_pairs={{0,16},{1,17},{2,18},{3,19},{4,20},{5,21},{6,22},{7,23},{8,24},{9,... | collective-permute-start | bytes 1572872 | tf_op jit(solution)/shard_map/ppermute | solution.py:209
  141.8 3.8 %collective-permute-start.7 = (bf16[2048,128]{1,0:T(8,128)(2,1)S(1)}, bf16[2048,128]{1,0:T(8,128)(2,1)S(1)}, u32[]{:S(2)}, u32[]{:S(2)}) collective-permute-start(bf16[2048,128]{1,0:T(8,128)(2,1)S(1)} %collective-permute-done.5.d1), channel_id=1, source_target_pairs={{0,16},{1,17},{2,18},{3,19},{4,20},{5,21},{6,22},{7,23},{8,24},{9,... | collective-permute-start | bytes 1572872 | tf_op jit(solution)/shard_map/ppermute | solution.py:209
  145.6 0.8 copy-start.5
  146.4 1.0 copy-start.6
  150.1 62.1 %all-to-all-start.3 = ((bf16[128,3,4,128]{3,2,1,0:T(4,128)(2,1)}), bf16[128,3,4,128]{3,2,1,0:T(4,128)(2,1)S(1)}, u32[]{:S(2)}, u32[]{:S(2)}) async-start(bf16[128,3,4,128]{3,2,1,0:T(4,128)(2,1)} %bitcast.10), calls=%async_computation.3 | async-start | bytes 786432 | tf_op jit(solution)/shard_map/all_to_all | solution.py:213

commit v3 on v2

--- a/solution.py
+++ b/solution.py
@@ -14,6 +14,8 @@
 SIDE = 4
 PLANE = SIDE * SIDE
 CAP = 12
+FIRST = 16
+STEP = 1
 TOK = 256
 ROWS = CHIPS * CAP
 UNIT = 2 * CAP
@@ -54,7 +56,7 @@
     rest = r - chip * UNIT
     half = rest >= CAP
     slot = jnp.where(half, rest - CAP, rest)
-    name = chip * SIDE + x
+    name = ((chip * STEP + FIRST) & (CHIPS - 1)) * SIDE + x
     named = name == ids_ref[0:1, :]
     for k in range(1, 4):
         named = named | (name == ids_ref[k : k + 1, :])
@@ -70,6 +72,8 @@
     r = iota(shape, 1)
     name = (r * 5462) >> 16
     slot = r - name * CAP
+    chip = ((name >> 2) * STEP + FIRST) & (CHIPS - 1)
+    name = chip * SIDE + (name & (SIDE - 1))
     named = jnp.zeros(shape, jnp.bool_)
     scale = jnp.zeros(shape, F32)
     for k in range(4):
@@ -195,10 +199,11 @@
 
 
 SIBLING = [(at(z, c, y, x), at(z, 1 - c, y, x)) for z, c, y, x in devices()]
-CORE_GROUPS = [[2 * z + c for z in range(CHIPS)] for c in range(2)]
+ORDER = [(i * STEP + FIRST) % CHIPS for i in range(CHIPS)]
+CORE_GROUPS = [[2 * z + c for z in ORDER] for c in range(2)]
 Y_GROUPS = [[SIDE * y + x for y in range(SIDE)] for x in range(SIDE)]
 BACK_GROUPS = [
-    [at(z, c, y, x) for z in range(CHIPS) for x in range(SIDE)]
+    [at(z, c, y, x) for z in ORDER for x in range(SIDE)]
     for c in range(2)
     for y in range(SIDE)
 ]

time: 214 us -> 205 us (0.958)
  the two profiles are of different devices: /device:TPU:14 before, /device:TPU:1 now
where the time goes in v3:
time: 205 us; the launch traced here: 204 us
  starting transfers between devices  98.5 us (48%)
  waiting for transfers between devices  79.1 us (39%)
  Pallas kernels  12.9 us (6%)
  local copies, waits for them, and re-layouts  10.6 us (5%)
  other arithmetic  2.2 us (1%)
    all_to_all x4, starting transfers between devices, exchange(): return lax.all_to_all(a, axes, 0, 0, tiled=True, axis_index_groups=groups)  69.8 us
    all_to_all x4, waiting for transfers between devices, exchange(): return lax.all_to_all(a, axes, 0, 0, tiled=True, axis_index_groups=groups)  63.1 us
    ppermute x8, starting transfers between devices, permute(): return lax.ppermute(a, BOTH, pairs)  28.7 us
    ppermute x8, waiting for transfers between devices, permute(): return lax.ppermute(a, BOTH, pairs)  16 us
    unnamed x34, local copies, waits for them, and re-layouts  9.13 us
    pallas_call x1, Pallas kernels, per_device(): call(gate_up_kernel, jax.ShapeDtypeStruct((SIDE, ROWS, BLOCK), BF), 7, 2...  4.79 us
  transfers between devices with their start and end apart: 12, of which 8 were waited for; matrix products, arithmetic and copies ran while one was open for 2% of the time, Pallas kernels for 1%

profile of v3, /device:TPU:1, one launch (start us, length us, event | category | flops | bytes accessed | tf_op | source)
XLA Modules:
  0.0 203.5 jit_solution(6824338417759255769)
XLA Ops:
  0.1 1.2 copy-done
  2.7 2.5 %shard_map.92 = bf16[768,256]{1,0:T(8,128)(2,1)} custom-call(s32[4]{0:T(128)S(1)} %pad_add_fusion.pos_ref, bf16[256,2048]{1,0:T(8,128)(2,1)S(1)} %copy-done, f32[1,2048]{1,0:T(1,128)S(1)} %bitcast.16, s32[4,256]{1,0:T(4,128)S(1)} %bitcast.15), custom_call_target="tpu_custom_call" | custom-call | flops 100000000 | bytes 2000000 | tf_op jit(solution)/shard_map/pallas_call | solution.py:225
  5.2 36.1 %all-to-all-start = ((bf16[32,24,256]{2,1,0:T(8,128)(2,1)}), bf16[32,24,256]{2,1,0:T(8,128)(2,1)S(1)}, u32[]{:S(2)}, u32[]{:S(2)}) async-start(bf16[32,24,256]{2,1,0:T(8,128)(2,1)} %bitcast.6), calls=%async_computation | async-start | bytes 786432 | tf_op jit(solution)/shard_map/all_to_all | solution.py:218
  41.6 1.1 pad_maximum_fusion
  42.6 5.8 %collective-permute-start = (bf16[2,2048,128]{2,1,0:T(8,128)(2,1)}, bf16[2,2048,128]{2,1,0:T(8,128)(2,1)S(1)}, u32[]{:S(2)}, u32[]{:S(2)}) collective-permute-start(bf16[2,2048,128]{2,1,0:T(8,128)(2,1)} %pad_maximum_fusion), channel_id=1, source_target_pairs={{0,0},{1,16},{2,1},{3,17},{4,4},{5,20},{6,5},{7,21},{8,8},{9,24},{... | collective-permute-start | bytes 3145736 | tf_op jit(solution)/shard_map/ppermute | solution.py:214
  48.4 1.1 pad_maximum_fusion.1
  49.5 1.9 collective-permute-start.1
  51.4 22.6 %all-to-all-done = bf16[32,24,256]{2,1,0:T(8,128)(2,1)S(1)} async-done(((bf16[32,24,256]{2,1,0:T(8,128)(2,1)}), bf16[32,24,256]{2,1,0:T(8,128)(2,1)S(1)}, u32[]{:S(2)}, u32[]{:S(2)}) %all-to-all-start) | async-done | bytes 393248 | tf_op jit(solution)/shard_map/all_to_all | solution.py:218
  74.0 1.3 broadcast_in_dim.8
  75.3 4.3 %all-to-all-start.1 = ((bf16[4,768,256]{2,1,0:T(8,128)(2,1)}), bf16[4,768,256]{2,1,0:T(8,128)(2,1)S(1)}, u32[]{:S(2)}, u32[]{:S(2)}) async-start(bf16[4,768,256]{2,1,0:T(8,128)(2,1)} %broadcast_in_dim.8), calls=%async_computation.1 | async-start | bytes 3145728 | tf_op jit(solution)/shard_map/all_to_all | solution.py:218
  79.6 4.9 %collective-permute-start.2 = (bf16[2,2048,128]{2,1,0:T(8,128)(2,1)S(1)}, bf16[2,2048,128]{2,1,0:T(8,128)(2,1)S(1)}, u32[]{:S(2)}, u32[]{:S(2)}) collective-permute-start(bf16[2,2048,128]{2,1,0:T(8,128)(2,1)S(1)} %collective-permute-done.w0), channel_id=1, source_target_pairs={{0,16},{1,17},{2,18},{3,19},{4,20},{5,21},{6,22},{7,23},{8,24},{9,... | collective-permute-start | bytes 3145736 | tf_op jit(solution)/shard_map/ppermute | solution.py:214
  84.6 1.9 collective-permute-start.3
  86.9 1.0 copy-done.1
  87.8 1.5 collective-permute-done.3.v1
  90.3 7.1 %all-to-all-done.1.raw_ref = bf16[4,768,256]{2,1,0:T(8,128)(2,1)S(1)} async-done(((bf16[4,768,256]{2,1,0:T(8,128)(2,1)}), bf16[4,768,256]{2,1,0:T(8,128)(2,1)S(1)}, u32[]{:S(2)}, u32[]{:S(2)}) %all-to-all-start.1) | async-done | bytes 1572896 | tf_op jit(solution)/shard_map/all_to_all | solution.py:218
  97.4 1.2 copy-done.2
  98.6 1.2 copy-done.4
  99.8 4.8 %shard_map.93 = bf16[4,384,512]{2,1,0:T(8,128)(2,1)} custom-call(s32[4]{0:T(128)S(1)} %pad_add_fusion.pos_ref, bf16[192,192]{1,0:T(8,128)(2,1)S(1)} %copy-done.7, bf16[4,768,256]{2,1,0:T(8,128)(2,1)S(1)} %all-to-all-done.1.raw_ref, bf16[2,2048,128]{2,1,0:T(8,128)(2,1)S(1)} %collective-permute-done.w0, bf16[2,2048,128]{2,1,0:T(8,128)(2,1)} %collective-permute-done.1.w1, ...), custom_call_target="tpu_custom_call" | custom-call | flops 2000000000 | bytes 6000000 | tf_op jit(solution)/shard_map/pallas_call | solution.py:255
  104.6 3.7 %all-to-all-start.2 = ((bf16[4,384,512]{2,1,0:T(8,128)(2,1)}), bf16[4,384,512]{2,1,0:T(8,128)(2,1)S(1)}, u32[]{:S(2)}, u32[]{:S(2)}) async-start(bf16[4,384,512]{2,1,0:T(8,128)(2,1)} %shard_map.93), calls=%async_computation.2 | async-start | bytes 3145728 | tf_op jit(solution)/shard_map/all_to_all | solution.py:218
  108.5 8.4 %collective-permute-start.4 = (bf16[2048,128]{1,0:T(8,128)(2,1)S(1)}, bf16[2048,128]{1,0:T(8,128)(2,1)S(1)}, u32[]{:S(2)}, u32[]{:S(2)}) collective-permute-start(bf16[2048,128]{1,0:T(8,128)(2,1)S(1)} %get-tuple-element.6), channel_id=1, source_target_pairs={{0,0},{1,16},{2,1},{3,17},{4,4},{5,20},{6,5},{7,21},{8,8},{9,24},{... | collective-permute-start | bytes 1572872 | tf_op jit(solution)/shard_map/ppermute | solution.py:214
  116.9 1.9 collective-permute-start.5
  118.9 8.9 %collective-permute-done.4.d0 = bf16[2048,128]{1,0:T(8,128)(2,1)S(1)} collective-permute-done((bf16[2048,128]{1,0:T(8,128)(2,1)S(1)}, bf16[2048,128]{1,0:T(8,128)(2,1)S(1)}, u32[]{:S(2)}, u32[]{:S(2)}) %collective-permute-start.4) | collective-permute-done | bytes 524320 | tf_op jit(solution)/shard_map/ppermute | solution.py:214
  127.7 1.9 collective-permute-start.6
  129.6 3.4 %collective-permute-done.5.d1 = bf16[2048,128]{1,0:T(8,128)(2,1)S(1)} collective-permute-done((bf16[2048,128]{1,0:T(8,128)(2,1)S(1)}, bf16[2048,128]{1,0:T(8,128)(2,1)S(1)}, u32[]{:S(2)}, u32[]{:S(2)}) %collective-permute-start.5) | collective-permute-done | bytes 524320 | tf_op jit(solution)/shard_map/ppermute | solution.py:214
  133.0 1.9 collective-permute-start.7
  135.0 1.9 collective-permute-done.7.e1
  137.6 1.0 copy-done.6
  138.7 2.7 %shard_map.94 = bf16[1536,128]{1,0:T(8,128)(2,1)} custom-call(s32[4]{0:T(128)S(1)} %pad_add_fusion.pos_ref, bf16[192,192]{1,0:T(8,128)(2,1)S(1)} %copy-done.8, bf16[4,384,512]{2,1,0:T(8,128)(2,1)S(1)} %all-to-all-done.2.acts, bf16[2048,128]{1,0:T(8,128)(2,1)S(1)} %collective-permute-done.4.d0, bf16[2048,128]{1,0:T(8,128)(2,1)S(1)} %collective-permute-done.5.d1, ...), custom_call_target="tpu_custom_call" | custom-call | flops 1000000000 | bytes 4000000 | tf_op jit(solution)/shard_map/pallas_call | solution.py:264
  141.3 25.6 %all-to-all-start.3 = ((bf16[128,3,4,128]{3,2,1,0:T(4,128)(2,1)}), bf16[128,3,4,128]{3,2,1,0:T(4,128)(2,1)S(1)}, u32[]{:S(2)}, u32[]{:S(2)}) async-start(bf16[128,3,4,128]{3,2,1,0:T(4,128)(2,1)} %bitcast.10), calls=%async_computation.3 | async-start | bytes 786432 | tf_op jit(solution)/shard_map/all_to_all | solution.py:218
  167.3 1.7 shard_map.91.scale_ref
  168.9 33.4 %all-to-all-done.3 = bf16[128,3,4,128]{3,2,1,0:T(4,128)(2,1)S(1)} async-done(((bf16[128,3,4,128]{3,2,1,0:T(4,128)(2,1)}), bf16[128,3,4,128]{3,2,1,0:T(4,128)(2,1)S(1)}, u32[]{:S(2)}, u32[]{:S(2)}) %all-to-all-start.3) | async-done | bytes 393248 | tf_op jit(solution)/shard_map/all_to_all | solution.py:218
  202.4 1.2 shard_map.95
  (37 shorter events, 4.1 us)
Async XLA Ops:
  0.1 1.2 copy-start
  1.3 0.7 copy-start.9
  2.0 0.7 copy-start.11
  2.7 38.7 %copy-start.12 = (bf16[2,2048,128]{2,1,0:T(8,128)(2,1)S(1)}, bf16[2,2048,128]{2,1,0:T(8,128)(2,1)}, u32[]{:S(2)}) copy-start(bf16[2,2048,128]{2,1,0:T(8,128)(2,1)} %param.14) | copy-start | bytes 3145732
  2.7 38.7 %copy-start.13 = (bf16[2,2048,128]{2,1,0:T(8,128)(2,1)S(1)}, bf16[2,2048,128]{2,1,0:T(8,128)(2,1)}, u32[]{:S(2)}) copy-start(bf16[2,2048,128]{2,1,0:T(8,128)(2,1)} %param.13) | copy-start | bytes 3145732
  5.2 68.8 %all-to-all-start = ((bf16[32,24,256]{2,1,0:T(8,128)(2,1)}), bf16[32,24,256]{2,1,0:T(8,128)(2,1)S(1)}, u32[]{:S(2)}, u32[]{:S(2)}) async-start(bf16[32,24,256]{2,1,0:T(8,128)(2,1)} %bitcast.6), calls=%async_computation | async-start | bytes 786432 | tf_op jit(solution)/shard_map/all_to_all | solution.py:218
  42.6 37.0 %collective-permute-start = (bf16[2,2048,128]{2,1,0:T(8,128)(2,1)}, bf16[2,2048,128]{2,1,0:T(8,128)(2,1)S(1)}, u32[]{:S(2)}, u32[]{:S(2)}) collective-permute-start(bf16[2,2048,128]{2,1,0:T(8,128)(2,1)} %pad_maximum_fusion), channel_id=1, source_target_pairs={{0,0},{1,16},{2,1},{3,17},{4,4},{5,20},{6,5},{7,21},{8,8},{9,24},{... | collective-permute-start | bytes 3145736 | tf_op jit(solution)/shard_map/ppermute | solution.py:214
  49.5 35.1 %collective-permute-start.1 = (bf16[2,2048,128]{2,1,0:T(8,128)(2,1)}, bf16[2,2048,128]{2,1,0:T(8,128)(2,1)}, u32[]{:S(2)}, u32[]{:S(2)}) collective-permute-start(bf16[2,2048,128]{2,1,0:T(8,128)(2,1)} %pad_maximum_fusion.1), channel_id=1, source_target_pairs={{0,1},{1,17},{2,0},{3,16},{4,5},{5,21},{6,4},{7,20},{8,9},{9,25},{... | collective-permute-start | bytes 3145736 | tf_op jit(solution)/shard_map/ppermute | solution.py:214
  75.3 22.1 %copy-start.7 = (bf16[192,192]{1,0:T(8,128)(2,1)S(1)}, bf16[192,192]{1,0:T(8,128)(2,1)}, u32[]{:S(2)}) copy-start(bf16[192,192]{1,0:T(8,128)(2,1)} %constant.35.clone.perm_ref) | copy-start | bytes 221188
  75.3 22.1 %all-to-all-start.1 = ((bf16[4,768,256]{2,1,0:T(8,128)(2,1)}), bf16[4,768,256]{2,1,0:T(8,128)(2,1)S(1)}, u32[]{:S(2)}, u32[]{:S(2)}) async-start(bf16[4,768,256]{2,1,0:T(8,128)(2,1)} %broadcast_in_dim.8), calls=%async_computation.1 | async-start | bytes 3145728 | tf_op jit(solution)/shard_map/all_to_all | solution.py:218
  79.6 7.2 %collective-permute-start.2 = (bf16[2,2048,128]{2,1,0:T(8,128)(2,1)S(1)}, bf16[2,2048,128]{2,1,0:T(8,128)(2,1)S(1)}, u32[]{:S(2)}, u32[]{:S(2)}) collective-permute-start(bf16[2,2048,128]{2,1,0:T(8,128)(2,1)S(1)} %collective-permute-done.w0), channel_id=1, source_target_pairs={{0,16},{1,17},{2,18},{3,19},{4,20},{5,21},{6,22},{7,23},{8,24},{9,... | collective-permute-start | bytes 3145736 | tf_op jit(solution)/shard_map/ppermute | solution.py:214
  84.6 4.8 %collective-permute-start.3 = (bf16[2,2048,128]{2,1,0:T(8,128)(2,1)}, bf16[2,2048,128]{2,1,0:T(8,128)(2,1)S(1)}, u32[]{:S(2)}, u32[]{:S(2)}) collective-permute-start(bf16[2,2048,128]{2,1,0:T(8,128)(2,1)} %collective-permute-done.1.w1), channel_id=1, source_target_pairs={{0,16},{1,17},{2,18},{3,19},{4,20},{5,21},{6,22},{7,23},{8,24},{9,... | collective-permute-start | bytes 3145736 | tf_op jit(solution)/shard_map/ppermute | solution.py:214
  86.9 1.0 copy-start.1
  89.4 1.0 copy-start.3
  97.4 1.2 copy-start.2
  98.6 1.2 copy-start.4
  104.6 3.7 %copy-start.14 = (bf16[2,2048,128]{2,1,0:T(8,128)(2,1)S(1)}, bf16[2,2048,128]{2,1,0:T(8,128)(2,1)}, u32[]{:S(2)}) copy-start(bf16[2,2048,128]{2,1,0:T(8,128)(2,1)} %param.15) | copy-start | bytes 3145732
  104.6 33.0 %all-to-all-start.2 = ((bf16[4,384,512]{2,1,0:T(8,128)(2,1)}), bf16[4,384,512]{2,1,0:T(8,128)(2,1)S(1)}, u32[]{:S(2)}, u32[]{:S(2)}) async-start(bf16[4,384,512]{2,1,0:T(8,128)(2,1)} %shard_map.93), calls=%async_computation.2 | async-start | bytes 3145728 | tf_op jit(solution)/shard_map/all_to_all | solution.py:218
  108.3 29.3 %copy-start.8 = (bf16[192,192]{1,0:T(8,128)(2,1)S(1)}, bf16[192,192]{1,0:T(8,128)(2,1)}, u32[]{:S(2)}) copy-start(bf16[192,192]{1,0:T(8,128)(2,1)} %constant.36.clone.perm_ref) | copy-start | bytes 221188
  108.4 58.6 %copy-start.10 = (s32[256,4]{0,1:T(4,128)S(1)}, s32[256,4]{0,1:T(4,128)}, u32[]{:S(2)}) copy-start(s32[256,4]{0,1:T(4,128)} %param.11) | copy-start | bytes 12292
  108.4 58.7 %copy-start.15 = (f32[256,4]{0,1:T(4,128)S(1)}, f32[256,4]{0,1:T(4,128)}, u32[]{:S(2)}) copy-start(f32[256,4]{0,1:T(4,128)} %param.12) | copy-start | bytes 12292
  108.5 19.3 %collective-permute-start.4 = (bf16[2048,128]{1,0:T(8,128)(2,1)S(1)}, bf16[2048,128]{1,0:T(8,128)(2,1)S(1)}, u32[]{:S(2)}, u32[]{:S(2)}) collective-permute-start(bf16[2048,128]{1,0:T(8,128)(2,1)S(1)} %get-tuple-element.6), channel_id=1, source_target_pairs={{0,0},{1,16},{2,1},{3,17},{4,4},{5,20},{6,5},{7,21},{8,8},{9,24},{... | collective-permute-start | bytes 1572872 | tf_op jit(solution)/shard_map/ppermute | solution.py:214
  116.9 16.1 %collective-permute-start.5 = (bf16[2048,128]{1,0:T(8,128)(2,1)S(1)}, bf16[2048,128]{1,0:T(8,128)(2,1)S(1)}, u32[]{:S(2)}, u32[]{:S(2)}) collective-permute-start(bf16[2048,128]{1,0:T(8,128)(2,1)S(1)} %get-tuple-element.5), channel_id=1, source_target_pairs={{0,1},{1,17},{2,0},{3,16},{4,5},{5,21},{6,4},{7,20},{8,9},{9,25},{... | collective-permute-start | bytes 1572872 | tf_op jit(solution)/shard_map/ppermute | solution.py:214
  127.7 7.2 %collective-permute-start.6 = (bf16[2048,128]{1,0:T(8,128)(2,1)S(1)}, bf16[2048,128]{1,0:T(8,128)(2,1)S(1)}, u32[]{:S(2)}, u32[]{:S(2)}) collective-permute-start(bf16[2048,128]{1,0:T(8,128)(2,1)S(1)} %collective-permute-done.4.d0), channel_id=1, source_target_pairs={{0,16},{1,17},{2,18},{3,19},{4,20},{5,21},{6,22},{7,23},{8,24},{9,... | collective-permute-start | bytes 1572872 | tf_op jit(solution)/shard_map/ppermute | solution.py:214
  133.0 3.8 %collective-permute-start.7 = (bf16[2048,128]{1,0:T(8,128)(2,1)S(1)}, bf16[2048,128]{1,0:T(8,128)(2,1)S(1)}, u32[]{:S(2)}, u32[]{:S(2)}) collective-permute-start(bf16[2048,128]{1,0:T(8,128)(2,1)S(1)} %collective-permute-done.5.d1), channel_id=1, source_target_pairs={{0,16},{1,17},{2,18},{3,19},{4,20},{5,21},{6,22},{7,23},{8,24},{9,... | collective-permute-start | bytes 1572872 | tf_op jit(solution)/shard_map/ppermute | solution.py:214
  136.8 0.8 copy-start.5
  137.6 1.0 copy-start.6
  141.3 61.0 %all-to-all-start.3 = ((bf16[128,3,4,128]{3,2,1,0:T(4,128)(2,1)}), bf16[128,3,4,128]{3,2,1,0:T(4,128)(2,1)S(1)}, u32[]{:S(2)}, u32[]{:S(2)}) async-start(bf16[128,3,4,128]{3,2,1,0:T(4,128)(2,1)} %bitcast.10), calls=%async_computation.3 | async-start | bytes 786432 | tf_op jit(solution)/shard_map/all_to_all | solution.py:218

commit v4 on v3

--- a/solution.py
+++ b/solution.py
@@ -14,7 +14,7 @@
 SIDE = 4
 PLANE = SIDE * SIDE
 CAP = 12
-FIRST = 16
+FIRST = 20
 STEP = 1
 TOK = 256
 ROWS = CHIPS * CAP
@@ -163,16 +163,16 @@
         ).astype(BF)
 
 
-def call(kernel, out_shape, n_in, flops, nbytes, scratch=(), scalars=True):
-    vmem = pl.BlockSpec(memory_space=pltpu.VMEM)
+def call(kernel, out_shape, n_in, flops, nbytes, scratch=(), scalars=True, vmem=24):
+    ref = pl.BlockSpec(memory_space=pltpu.VMEM)
     first = [pl.BlockSpec(memory_space=pltpu.SMEM)] if scalars else []
     return pl.pallas_call(
         kernel,
         out_shape=out_shape,
-        in_specs=first + [vmem] * (n_in - len(first)),
-        out_specs=jax.tree.map(lambda _: vmem, out_shape),
+        in_specs=first + [ref] * (n_in - len(first)),
+        out_specs=jax.tree.map(lambda _: ref, out_shape),
         scratch_shapes=list(scratch),
-        compiler_params=pltpu.CompilerParams(vmem_limit_bytes=24 * 2**20),
+        compiler_params=pltpu.CompilerParams(vmem_limit_bytes=vmem * 2**20),
         cost_estimate=pl.CostEstimate(
             flops=flops, bytes_accessed=nbytes, transcendentals=0
         ),
@@ -223,7 +223,12 @@
     x, z, core = tp & 3, ep >> 1, ep & 1
     pos = jnp.stack([core, x, z, tp >> 2]).astype(jnp.int32)
     outgoing = call(
-        prep_kernel, jax.ShapeDtypeStruct((CHIPS * UNIT, HALF), BF), 4, 10**8, 2 * 10**6
+        prep_kernel,
+        jax.ShapeDtypeStruct((CHIPS * UNIT, HALF), BF),
+        4,
+        10**8,
+        2 * 10**6,
+        vmem=60,
     )(pos, tokens, norm_gain.reshape(1, -1), route_ids.T)
     raw = exchange(outgoing.reshape(CHIPS, UNIT, HALF), "ep", CORE_GROUPS)
 

time: 205 us -> 203 us (level)
  starting transfers between devices: 98.5 us -> 86.4 us
  waiting for transfers between devices: 79.1 us -> 89.9 us
  local copies, waits for them, and re-layouts: 10.6 us -> 8.13 us
    all_to_all x4, waiting for transfers between devices: 63.1 us -> 73.9 us  [exchange(): return lax.all_to_all(a, axes, 0, 0, tiled=True, axis_index_groups=groups)]
    all_to_all x4, starting transfers between devices: 69.8 us -> 60.1 us  [exchange(): return lax.all_to_all(a, axes, 0, 0, tiled=True, axis_index_groups=groups)]
    unnamed x34 -> x30, local copies, waits for them, and re-layouts: 9.13 us -> 6.55 us
    ppermute x8, starting transfers between devices: 28.7 us -> 26.3 us  [permute(): return lax.ppermute(a, BOTH, pairs)]
where the time goes in v4:
time: 203 us; the launch traced here: 201 us
  waiting for transfers between devices  89.9 us (44%)
  starting transfers between devices  86.4 us (43%)
  Pallas kernels  13.7 us (7%)
  local copies, waits for them, and re-layouts  8.13 us (4%)
  other arithmetic  2.76 us (1%)
    all_to_all x4, waiting for transfers between devices, exchange(): return lax.all_to_all(a, axes, 0, 0, tiled=True, axis_index_groups=groups)  73.9 us
    all_to_all x4, starting transfers between devices, exchange(): return lax.all_to_all(a, axes, 0, 0, tiled=True, axis_index_groups=groups)  60.1 us
    ppermute x8, starting transfers between devices, permute(): return lax.ppermute(a, BOTH, pairs)  26.3 us
    ppermute x8, waiting for transfers between devices, permute(): return lax.ppermute(a, BOTH, pairs)  16 us
    unnamed x30, local copies, waits for them, and re-layouts  6.55 us
    pallas_call x1, Pallas kernels, per_device(): call(gate_up_kernel, jax.ShapeDtypeStruct((SIDE, ROWS, BLOCK), BF), 7, 2...  4.8 us
  transfers between devices with their start and end apart: 12, of which 8 were waited for; matrix products, arithmetic and copies ran while one was open for 2% of the time, Pallas kernels for 1%

profile of v4, /device:TPU:1, one launch (start us, length us, event | category | flops | bytes accessed | tf_op | source)
XLA Modules:
  0.0 201.1 jit_solution(6855577289344753425)
XLA Ops:
  0.6 3.3 %shard_map.92 = bf16[768,256]{1,0:T(8,128)(2,1)} custom-call(s32[4]{0:T(128)} %pad_add_fusion.pos_ref, bf16[256,2048]{1,0:T(8,128)(2,1)} %tok_ref.1, f32[1,2048]{1,0:T(1,128)} %bitcast.18, s32[4,256]{1,0:T(4,128)} %bitcast.17), custom_call_target="tpu_custom_call" | custom-call | flops 100000000 | bytes 2000000 | tf_op jit(solution)/shard_map/pallas_call | solution.py:225
  3.9 31.3 %all-to-all-start = ((bf16[32,24,256]{2,1,0:T(8,128)(2,1)}), bf16[32,24,256]{2,1,0:T(8,128)(2,1)S(1)}, u32[]{:S(2)}, u32[]{:S(2)}) async-start(bf16[32,24,256]{2,1,0:T(8,128)(2,1)} %bitcast.15), calls=%async_computation | async-start | bytes 786432 | tf_op jit(solution)/shard_map/all_to_all | solution.py:218
  35.5 1.1 pad_maximum_fusion
  36.6 5.8 %collective-permute-start = (bf16[2,2048,128]{2,1,0:T(8,128)(2,1)}, bf16[2,2048,128]{2,1,0:T(8,128)(2,1)S(1)}, u32[]{:S(2)}, u32[]{:S(2)}) collective-permute-start(bf16[2,2048,128]{2,1,0:T(8,128)(2,1)} %pad_maximum_fusion), channel_id=1, source_target_pairs={{0,0},{1,16},{2,1},{3,17},{4,4},{5,20},{6,5},{7,21},{8,8},{9,24},{... | collective-permute-start | bytes 3145736 | tf_op jit(solution)/shard_map/ppermute | solution.py:214
  42.3 1.1 pad_maximum_fusion.1
  43.4 1.9 collective-permute-start.1
  45.3 27.3 %all-to-all-done = bf16[32,24,256]{2,1,0:T(8,128)(2,1)S(1)} async-done(((bf16[32,24,256]{2,1,0:T(8,128)(2,1)}), bf16[32,24,256]{2,1,0:T(8,128)(2,1)S(1)}, u32[]{:S(2)}, u32[]{:S(2)}) %all-to-all-start) | async-done | bytes 393248 | tf_op jit(solution)/shard_map/all_to_all | solution.py:218
  72.6 1.3 broadcast_in_dim.8
  73.9 4.3 %all-to-all-start.1 = ((bf16[4,768,256]{2,1,0:T(8,128)(2,1)}), bf16[4,768,256]{2,1,0:T(8,128)(2,1)S(1)}, u32[]{:S(2)}, u32[]{:S(2)}) async-start(bf16[4,768,256]{2,1,0:T(8,128)(2,1)} %broadcast_in_dim.8), calls=%async_computation.1 | async-start | bytes 3145728 | tf_op jit(solution)/shard_map/all_to_all | solution.py:218
  78.2 3.7 %collective-permute-start.2 = (bf16[2,2048,128]{2,1,0:T(8,128)(2,1)S(1)}, bf16[2,2048,128]{2,1,0:T(8,128)(2,1)S(1)}, u32[]{:S(2)}, u32[]{:S(2)}) collective-permute-start(bf16[2,2048,128]{2,1,0:T(8,128)(2,1)S(1)} %collective-permute-done.w0), channel_id=1, source_target_pairs={{0,16},{1,17},{2,18},{3,19},{4,20},{5,21},{6,22},{7,23},{8,24},{9,... | collective-permute-start | bytes 3145736 | tf_op jit(solution)/shard_map/ppermute | solution.py:214
  82.0 1.9 collective-permute-start.3
  84.2 1.0 copy-done
  85.2 1.5 collective-permute-done.3.v1
  86.7 1.0 copy-done.2
  87.7 9.5 %all-to-all-done.1.raw_ref = bf16[4,768,256]{2,1,0:T(8,128)(2,1)S(1)} async-done(((bf16[4,768,256]{2,1,0:T(8,128)(2,1)}), bf16[4,768,256]{2,1,0:T(8,128)(2,1)S(1)}, u32[]{:S(2)}, u32[]{:S(2)}) %all-to-all-start.1) | async-done | bytes 1572896 | tf_op jit(solution)/shard_map/all_to_all | solution.py:218
  97.2 1.2 copy-done.1
  98.4 1.2 copy-done.3
  99.6 4.8 %shard_map.93 = bf16[4,384,512]{2,1,0:T(8,128)(2,1)} custom-call(s32[4]{0:T(128)S(1)} %copy-done.8, bf16[192,192]{1,0:T(8,128)(2,1)S(1)} %copy-done.6, bf16[4,768,256]{2,1,0:T(8,128)(2,1)S(1)} %all-to-all-done.1.raw_ref, bf16[2,2048,128]{2,1,0:T(8,128)(2,1)S(1)} %collective-permute-done.w0, bf16[2,2048,128]{2,1,0:T(8,128)(2,1)} %collective-permute-done.1.w1, ...), custom_call_target="tpu_custom_call" | custom-call | flops 2000000000 | bytes 6000000 | tf_op jit(solution)/shard_map/pallas_call | solution.py:260
  104.4 3.7 %all-to-all-start.2 = ((bf16[4,384,512]{2,1,0:T(8,128)(2,1)}), bf16[4,384,512]{2,1,0:T(8,128)(2,1)S(1)}, u32[]{:S(2)}, u32[]{:S(2)}) async-start(bf16[4,384,512]{2,1,0:T(8,128)(2,1)} %shard_map.93), calls=%async_computation.2 | async-start | bytes 3145728 | tf_op jit(solution)/shard_map/all_to_all | solution.py:218
  108.3 7.2 %collective-permute-start.4 = (bf16[2048,128]{1,0:T(8,128)(2,1)S(1)}, bf16[2048,128]{1,0:T(8,128)(2,1)S(1)}, u32[]{:S(2)}, u32[]{:S(2)}) collective-permute-start(bf16[2048,128]{1,0:T(8,128)(2,1)S(1)} %get-tuple-element.6), channel_id=1, source_target_pairs={{0,0},{1,16},{2,1},{3,17},{4,4},{5,20},{6,5},{7,21},{8,8},{9,24},{... | collective-permute-start | bytes 1572872 | tf_op jit(solution)/shard_map/ppermute | solution.py:214
  115.5 1.9 collective-permute-start.5
  117.4 9.0 %collective-permute-done.4.d0 = bf16[2048,128]{1,0:T(8,128)(2,1)S(1)} collective-permute-done((bf16[2048,128]{1,0:T(8,128)(2,1)S(1)}, bf16[2048,128]{1,0:T(8,128)(2,1)S(1)}, u32[]{:S(2)}, u32[]{:S(2)}) %collective-permute-start.4) | collective-permute-done | bytes 524320 | tf_op jit(solution)/shard_map/ppermute | solution.py:214
  126.5 1.9 collective-permute-start.6
  128.4 3.2 %collective-permute-done.5.d1 = bf16[2048,128]{1,0:T(8,128)(2,1)S(1)} collective-permute-done((bf16[2048,128]{1,0:T(8,128)(2,1)S(1)}, bf16[2048,128]{1,0:T(8,128)(2,1)S(1)}, u32[]{:S(2)}, u32[]{:S(2)}) %collective-permute-start.5) | collective-permute-done | bytes 524320 | tf_op jit(solution)/shard_map/ppermute | solution.py:214
  131.6 1.9 collective-permute-start.7
  133.6 1.9 collective-permute-done.7.e1
  136.2 1.0 copy-done.5
  137.3 2.7 %shard_map.94 = bf16[1536,128]{1,0:T(8,128)(2,1)} custom-call(s32[4]{0:T(128)S(1)} %copy-done.8, bf16[192,192]{1,0:T(8,128)(2,1)S(1)} %copy-done.7, bf16[4,384,512]{2,1,0:T(8,128)(2,1)S(1)} %all-to-all-done.2.acts, bf16[2048,128]{1,0:T(8,128)(2,1)S(1)} %collective-permute-done.4.d0, bf16[2048,128]{1,0:T(8,128)(2,1)S(1)} %collective-permute-done.5.d1, ...), custom_call_target="tpu_custom_call" | custom-call | flops 1000000000 | bytes 4000000 | tf_op jit(solution)/shard_map/pallas_call | solution.py:269
  140.0 20.8 %all-to-all-start.3 = ((bf16[128,3,4,128]{3,2,1,0:T(4,128)(2,1)}), bf16[128,3,4,128]{3,2,1,0:T(4,128)(2,1)S(1)}, u32[]{:S(2)}, u32[]{:S(2)}) async-start(bf16[128,3,4,128]{3,2,1,0:T(4,128)(2,1)} %bitcast.10), calls=%async_computation.3 | async-start | bytes 786432 | tf_op jit(solution)/shard_map/all_to_all | solution.py:218
  161.1 1.7 shard_map.91.scale_ref
  162.8 37.2 %all-to-all-done.3 = bf16[128,3,4,128]{3,2,1,0:T(4,128)(2,1)S(1)} async-done(((bf16[128,3,4,128]{3,2,1,0:T(4,128)(2,1)}), bf16[128,3,4,128]{3,2,1,0:T(4,128)(2,1)S(1)}, u32[]{:S(2)}, u32[]{:S(2)}) %all-to-all-start.3) | async-done | bytes 393248 | tf_op jit(solution)/shard_map/all_to_all | solution.py:218
  199.9 1.2 shard_map.95
  (33 shorter events, 2.3 us)
Async XLA Ops:
  0.0 35.3 %copy-start.10 = (bf16[2,2048,128]{2,1,0:T(8,128)(2,1)S(1)}, bf16[2,2048,128]{2,1,0:T(8,128)(2,1)}, u32[]{:S(2)}) copy-start(bf16[2,2048,128]{2,1,0:T(8,128)(2,1)} %param.13) | copy-start | bytes 3145732
  0.0 35.3 %copy-start.9 = (bf16[2,2048,128]{2,1,0:T(8,128)(2,1)S(1)}, bf16[2,2048,128]{2,1,0:T(8,128)(2,1)}, u32[]{:S(2)}) copy-start(bf16[2,2048,128]{2,1,0:T(8,128)(2,1)} %param.14) | copy-start | bytes 3145732
  3.9 68.7 %all-to-all-start = ((bf16[32,24,256]{2,1,0:T(8,128)(2,1)}), bf16[32,24,256]{2,1,0:T(8,128)(2,1)S(1)}, u32[]{:S(2)}, u32[]{:S(2)}) async-start(bf16[32,24,256]{2,1,0:T(8,128)(2,1)} %bitcast.15), calls=%async_computation | async-start | bytes 786432 | tf_op jit(solution)/shard_map/all_to_all | solution.py:218
  36.6 41.6 %collective-permute-start = (bf16[2,2048,128]{2,1,0:T(8,128)(2,1)}, bf16[2,2048,128]{2,1,0:T(8,128)(2,1)S(1)}, u32[]{:S(2)}, u32[]{:S(2)}) collective-permute-start(bf16[2,2048,128]{2,1,0:T(8,128)(2,1)} %pad_maximum_fusion), channel_id=1, source_target_pairs={{0,0},{1,16},{2,1},{3,17},{4,4},{5,20},{6,5},{7,21},{8,8},{9,24},{... | collective-permute-start | bytes 3145736 | tf_op jit(solution)/shard_map/ppermute | solution.py:214
  43.4 38.6 %collective-permute-start.1 = (bf16[2,2048,128]{2,1,0:T(8,128)(2,1)}, bf16[2,2048,128]{2,1,0:T(8,128)(2,1)}, u32[]{:S(2)}, u32[]{:S(2)}) collective-permute-start(bf16[2,2048,128]{2,1,0:T(8,128)(2,1)} %pad_maximum_fusion.1), channel_id=1, source_target_pairs={{0,1},{1,17},{2,0},{3,16},{4,5},{5,21},{6,4},{7,20},{8,9},{9,25},{... | collective-permute-start | bytes 3145736 | tf_op jit(solution)/shard_map/ppermute | solution.py:214
  73.9 23.3 %copy-start.6 = (bf16[192,192]{1,0:T(8,128)(2,1)S(1)}, bf16[192,192]{1,0:T(8,128)(2,1)}, u32[]{:S(2)}) copy-start(bf16[192,192]{1,0:T(8,128)(2,1)} %constant.35.clone.perm_ref) | copy-start | bytes 221188
  73.9 23.3 %copy-start.8 = (s32[4]{0:T(128)S(1)}, s32[4]{0:T(128)}, u32[]{:S(2)}) copy-start(s32[4]{0:T(128)} %pad_add_fusion.pos_ref) | copy-start | bytes 52
  73.9 23.3 %all-to-all-start.1 = ((bf16[4,768,256]{2,1,0:T(8,128)(2,1)}), bf16[4,768,256]{2,1,0:T(8,128)(2,1)S(1)}, u32[]{:S(2)}, u32[]{:S(2)}) async-start(bf16[4,768,256]{2,1,0:T(8,128)(2,1)} %broadcast_in_dim.8), calls=%async_computation.1 | async-start | bytes 3145728 | tf_op jit(solution)/shard_map/all_to_all | solution.py:218
  78.2 6.0 %collective-permute-start.2 = (bf16[2,2048,128]{2,1,0:T(8,128)(2,1)S(1)}, bf16[2,2048,128]{2,1,0:T(8,128)(2,1)S(1)}, u32[]{:S(2)}, u32[]{:S(2)}) collective-permute-start(bf16[2,2048,128]{2,1,0:T(8,128)(2,1)S(1)} %collective-permute-done.w0), channel_id=1, source_target_pairs={{0,16},{1,17},{2,18},{3,19},{4,20},{5,21},{6,22},{7,23},{8,24},{9,... | collective-permute-start | bytes 3145736 | tf_op jit(solution)/shard_map/ppermute | solution.py:214
  82.0 4.8 %collective-permute-start.3 = (bf16[2,2048,128]{2,1,0:T(8,128)(2,1)}, bf16[2,2048,128]{2,1,0:T(8,128)(2,1)S(1)}, u32[]{:S(2)}, u32[]{:S(2)}) collective-permute-start(bf16[2,2048,128]{2,1,0:T(8,128)(2,1)} %collective-permute-done.1.w1), channel_id=1, source_target_pairs={{0,16},{1,17},{2,18},{3,19},{4,20},{5,21},{6,22},{7,23},{8,24},{9,... | collective-permute-start | bytes 3145736 | tf_op jit(solution)/shard_map/ppermute | solution.py:214
  84.2 1.0 copy-start
  86.7 1.0 copy-start.2
  97.2 1.2 copy-start.1
  98.4 1.2 copy-start.3
  104.4 3.7 %copy-start.11 = (bf16[2,2048,128]{2,1,0:T(8,128)(2,1)S(1)}, bf16[2,2048,128]{2,1,0:T(8,128)(2,1)}, u32[]{:S(2)}) copy-start(bf16[2,2048,128]{2,1,0:T(8,128)(2,1)} %param.15) | copy-start | bytes 3145732
  104.4 31.8 %all-to-all-start.2 = ((bf16[4,384,512]{2,1,0:T(8,128)(2,1)}), bf16[4,384,512]{2,1,0:T(8,128)(2,1)S(1)}, u32[]{:S(2)}, u32[]{:S(2)}) async-start(bf16[4,384,512]{2,1,0:T(8,128)(2,1)} %shard_map.93), calls=%async_computation.2 | async-start | bytes 3145728 | tf_op jit(solution)/shard_map/all_to_all | solution.py:218
  108.2 28.1 %copy-start.7 = (bf16[192,192]{1,0:T(8,128)(2,1)S(1)}, bf16[192,192]{1,0:T(8,128)(2,1)}, u32[]{:S(2)}) copy-start(bf16[192,192]{1,0:T(8,128)(2,1)} %constant.36.clone.perm_ref) | copy-start | bytes 221188
  108.2 52.6 %copy-start.12 = (s32[256,4]{0,1:T(4,128)S(1)}, s32[256,4]{0,1:T(4,128)}, u32[]{:S(2)}) copy-start(s32[256,4]{0,1:T(4,128)} %param.11) | copy-start | bytes 12292
  108.2 52.7 %copy-start.13 = (f32[256,4]{0,1:T(4,128)S(1)}, f32[256,4]{0,1:T(4,128)}, u32[]{:S(2)}) copy-start(f32[256,4]{0,1:T(4,128)} %param.12) | copy-start | bytes 12292
  108.3 18.2 %collective-permute-start.4 = (bf16[2048,128]{1,0:T(8,128)(2,1)S(1)}, bf16[2048,128]{1,0:T(8,128)(2,1)S(1)}, u32[]{:S(2)}, u32[]{:S(2)}) collective-permute-start(bf16[2048,128]{1,0:T(8,128)(2,1)S(1)} %get-tuple-element.6), channel_id=1, source_target_pairs={{0,0},{1,16},{2,1},{3,17},{4,4},{5,20},{6,5},{7,21},{8,8},{9,24},{... | collective-permute-start | bytes 1572872 | tf_op jit(solution)/shard_map/ppermute | solution.py:214
  115.5 16.1 %collective-permute-start.5 = (bf16[2048,128]{1,0:T(8,128)(2,1)S(1)}, bf16[2048,128]{1,0:T(8,128)(2,1)S(1)}, u32[]{:S(2)}, u32[]{:S(2)}) collective-permute-start(bf16[2048,128]{1,0:T(8,128)(2,1)S(1)} %get-tuple-element.5), channel_id=1, source_target_pairs={{0,1},{1,17},{2,0},{3,16},{4,5},{5,21},{6,4},{7,20},{8,9},{9,25},{... | collective-permute-start | bytes 1572872 | tf_op jit(solution)/shard_map/ppermute | solution.py:214
  126.5 7.1 %collective-permute-start.6 = (bf16[2048,128]{1,0:T(8,128)(2,1)S(1)}, bf16[2048,128]{1,0:T(8,128)(2,1)S(1)}, u32[]{:S(2)}, u32[]{:S(2)}) collective-permute-start(bf16[2048,128]{1,0:T(8,128)(2,1)S(1)} %collective-permute-done.4.d0), channel_id=1, source_target_pairs={{0,16},{1,17},{2,18},{3,19},{4,20},{5,21},{6,22},{7,23},{8,24},{9,... | collective-permute-start | bytes 1572872 | tf_op jit(solution)/shard_map/ppermute | solution.py:214
  131.6 3.8 %collective-permute-start.7 = (bf16[2048,128]{1,0:T(8,128)(2,1)S(1)}, bf16[2048,128]{1,0:T(8,128)(2,1)S(1)}, u32[]{:S(2)}, u32[]{:S(2)}) collective-permute-start(bf16[2048,128]{1,0:T(8,128)(2,1)S(1)} %collective-permute-done.5.d1), channel_id=1, source_target_pairs={{0,16},{1,17},{2,18},{3,19},{4,20},{5,21},{6,22},{7,23},{8,24},{9,... | collective-permute-start | bytes 1572872 | tf_op jit(solution)/shard_map/ppermute | solution.py:214
  135.4 0.8 copy-start.4
  136.2 1.0 copy-start.5
  140.0 60.0 %all-to-all-start.3 = ((bf16[128,3,4,128]{3,2,1,0:T(4,128)(2,1)}), bf16[128,3,4,128]{3,2,1,0:T(4,128)(2,1)S(1)}, u32[]{:S(2)}, u32[]{:S(2)}) async-start(bf16[128,3,4,128]{3,2,1,0:T(4,128)(2,1)} %bitcast.10), calls=%async_computation.3 | async-start | bytes 786432 | tf_op jit(solution)/shard_map/all_to_all | solution.py:218
